TPU v7x, 32 devices: a whole 2x2x4 slice. The times are simulated.
32 devices in a mesh: sp: 8 (over z, core), tp: 4 (over y, x).
Axes of the slice: x: 2, y: 2, z: 4, core: 2. Of those that a mesh axis runs over, the one named last changes fastest.
Arguments:
- rec_input: bfloat16 [3072, 3072], P('sp', 'tp'), may hold values from -6 to 6
- gate_input: bfloat16 [3072, 3072], P('sp', 'tp'), may hold values from -6 to 6
- conv_weight: bfloat16 [4, 3072], P(None, 'tp'), may hold values from -3 to 3
- decay_wide: bfloat16 [2, 16, 128, 128], P(None, 'tp'), may hold values from -0.5 to 0.5
- decay_narrow: bfloat16 [2, 16, 64, 64], P(None, 'tp'), may hold values from -0.75 to 0.75
- input_wide: bfloat16 [2, 16, 128, 128], P(None, 'tp'), may hold values from -0.5 to 0.5
- input_narrow: bfloat16 [2, 16, 64, 64], P(None, 'tp'), may hold values from -0.75 to 0.75
- decay_base: float32 [2, 3072], P(None, 'tp'), may hold values from 6.510417e-06 to 8.138021e-05
- decay_extra: float32 [2, 3072, 2, 16], P(None, 'sp', None, 'tp'), may hold values from -1 to 0
- tokens: bfloat16 [3072, 2048], P('sp', 'tp'), may hold values from -16 to 16
- out_weight: bfloat16 [3072, 2048], P(None, 'tp'), may hold values from -0.3125 to 0.3125
- norm_gain: float32 [2048], P('tp'), may hold values from 0.1 to 1.9
- shared_gate: bfloat16 [2048, 2048], P(None, 'tp'), may hold values from -0.125 to 0.125
- shared_up: bfloat16 [2048, 2048], P(None, 'tp'), may hold values from -0.125 to 0.125
- shared_down: bfloat16 [2048, 2048], P(None, 'tp'), may hold values from -0.125 to 0.125
- expert_gate: bfloat16 [8, 2048, 2048], P('sp', None, 'tp'), may hold values from -0.125 to 0.125
- expert_up: bfloat16 [8, 2048, 2048], P('sp', None, 'tp'), may hold values from -0.125 to 0.125
- expert_down: bfloat16 [8, 2048, 2048], P('sp', None, 'tp'), may hold values from -0.125 to 0.125
- routes: int32 [3072, 2], P('sp'), may hold values from 0 to 7, all different within a row; in each aligned block of 384 rows (0 to 383, 384 to 767, ...) at most 144 rows name the same one
- route_weight: float32 [3072, 2], P('sp'), may hold values from 0.2 to 1.5
Outputs:
- layer_out: bfloat16 [3072, 2048], P('sp', 'tp')
Inputs may be any that keep to these rules, and one draw needn't show every extreme that they name: `routes`: each row names 2 different experts. The rows of one index of sp name no expert more than 144 times, and in some such block one expert exactly 144 times.
All inputs are finite; a program needn't handle non-finite values.
Results may differ from a plain program's by a relative error of at most 0.0052.
Values may be sent and summed in bfloat16 or wider, within the bound.
A program may use at most 64 MiB of HBM per device.

v0:
```python
import functools

import jax
import jax.numpy as jnp
import numpy as np
from jax import lax
from jax.experimental import pallas as pl
from jax.experimental.pallas import tpu as pltpu
from jax.sharding import PartitionSpec as P

MESH = pl.DeviceIdType.MESH
D = 2048
CONV = 4
NORM_EPS = 1e-06
RATE_SCALE = 8.0
SEG = 8
F32 = jnp.float32
BF16 = jnp.bfloat16
EXACT = lax.Precision.HIGHEST


def rcopy(src, dst, send, recv, **where):
    return pltpu.make_async_remote_copy(
        src_ref=src, dst_ref=dst, send_sem=send, recv_sem=recv, device_id=where, device_id_type=MESH
    )


def greet(n_sp, n_tp):
    sp, tp = lax.axis_index("sp"), lax.axis_index("tp")
    barrier = pltpu.get_barrier_semaphore()
    for k in range(1, n_sp):
        pl.semaphore_signal(
            barrier, inc=1, device_id={"sp": lax.rem(sp + k, n_sp)}, device_id_type=MESH
        )
    for k in range(1, n_tp):
        pl.semaphore_signal(
            barrier, inc=1, device_id={"tp": lax.rem(tp + k, n_tp)}, device_id_type=MESH
        )
    pl.semaphore_wait(barrier, n_sp + n_tp - 2)


def gather_sems(n_tp):
    count = 6 if n_tp == 4 else n_tp
    return [pltpu.SemaphoreType.DMA((count,)), pltpu.SemaphoreType.DMA((count,))]


class Gather:
    def __init__(self, n_tp, slot, send, recv, base=0):
        self.n, self.slot, self.send, self.recv, self.base = n_tp, slot, send, recv, base
        self.t = lax.axis_index("tp")
        if n_tp == 4:
            y, x = self.t // 2, lax.rem(self.t, 2)
            self.xn, self.yn, self.dg = y * 2 + 1 - x, (1 - y) * 2 + x, 3 - self.t

    def piece(self, owner, half, sem, to):
        ref = self.slot(owner, half)
        s = self.base + sem
        return rcopy(ref, ref, self.send.at[s], self.recv.at[s], tp=to)

    def start(self):
        if self.n == 4:
            self.piece(self.t, 0, 0, self.xn).start()
            self.piece(self.t, 1, 3, self.yn).start()
            self.piece(self.t, 1, 1, self.xn).start()
            self.piece(self.t, 0, 2, self.yn).start()
        else:
            for k in range(1, self.n):
                to = lax.rem(self.t + k, self.n)
                self.piece(self.t, None, k, to).start()

    def forward(self):
        if self.n == 4:
            self.piece(self.xn, 0, 0, self.xn).wait_recv()
            self.piece(self.xn, 0, 4, self.yn).start()
            self.piece(self.yn, 1, 3, self.yn).wait_recv()
            self.piece(self.yn, 1, 5, self.xn).start()

    def arrivals(self):
        if self.n == 4:
            self.piece(self.xn, 1, 1, self.xn).wait_recv()
            yield self.xn
            self.piece(self.yn, 0, 2, self.yn).wait_recv()
            yield self.yn
            self.piece(self.dg, 0, 4, self.yn).wait_recv()
            self.piece(self.dg, 1, 5, self.xn).wait_recv()
            yield self.dg
        else:
            for k in range(1, self.n):
                owner = lax.rem(self.t - k + self.n, self.n)
                self.piece(owner, None, k, owner).wait_recv()
                yield owner

    def drain(self):
        if self.n == 4:
            for s, half, owner in (
                (0, 0, self.t), (1, 1, self.t), (2, 0, self.t), (3, 1, self.t),
                (4, 0, self.xn), (5, 1, self.yn),
            ):
                self.piece(owner, half, s, self.xn).wait_send()
        else:
            for k in range(1, self.n):
                to = lax.rem(self.t + k, self.n)
                self.piece(self.t, None, k, to).wait_send()


def minus_expm1(y):
    series = 1.0 + y * (1 / 7.0)
    for d in (6.0, 5.0, 4.0, 3.0, 2.0):
        series = 1.0 + y * (1 / d) * series
    return jnp.where(y > -0.3, -y * series, 1.0 - jnp.exp(y))


def front_kernel(
    n_sp, n_tp,
    rec, gate, convw, wblk, base, extra, spread, perm, permt, tokens, hbm_outw, gain,
    resid, whole, normed,
    halo, cperm, gperm, av, bv, msg, totals, mixedp, mixed, squares, sqown,
    hsend, hrecv, tsend, trecv, gsend, grecv, ssend, srecv, nsend, nrecv, outw, wsem,
):
    rows, chan = rec.shape
    groups, gw = wblk.shape[1], wblk.shape[2]
    cols = tokens.shape[1]
    seglen = rows // SEG
    sp, tp = lax.axis_index("sp"), lax.axis_index("tp")
    load = pltpu.make_async_copy(hbm_outw, outw, wsem.at[0])
    load.start()
    greet(n_sp, n_tp)
    up, down = lax.rem(sp + 1, n_sp), lax.rem(sp + n_sp - 1, n_sp)
    low = rcopy(rec.at[pl.ds(rows - 16, 16)], halo.at[0], hsend.at[0], hrecv.at[0], sp=up)
    high = rcopy(rec.at[pl.ds(0, 16)], halo.at[1], hsend.at[1], hrecv.at[1], sp=down)
    low.start()
    high.start()

    gperm[...] = jnp.dot(permt[...], gate[...], preferred_element_type=F32).astype(BF16)
    low.wait()
    high.wait()
    x = rec[...].astype(F32)
    lo = jnp.where(sp > 0, halo[0].astype(F32), 0.0)
    hi = jnp.where(sp < n_sp - 1, halo[1].astype(F32), 0.0)
    padded = jnp.concatenate([lo[14:16], x, hi[0:1]], axis=0)
    conv = padded[0:rows] * convw[0:1, :]
    for j in range(1, CONV):
        conv = conv + padded[j : j + rows] * convw[j : j + 1, :]
    cperm[...] = jnp.dot(
        permt[...], conv.astype(BF16), preferred_element_type=F32
    ).astype(BF16)

    step = 64

    @pl.loop(0, rows // step)
    def _(r):
        at = pl.ds(pl.multiple_of(r * step, step), step)
        for d in range(2):
            ex = jnp.dot(extra[d, at, :], spread[...], precision=EXACT, preferred_element_type=F32)
            for g in range(groups):
                lanes = slice(g * gw, (g + 1) * gw)
                c = cperm[at, lanes]
                rate = jax.nn.sigmoid(jnp.dot(c, wblk[2 * d, g], preferred_element_type=F32))
                admit = jax.nn.sigmoid(jnp.dot(c, wblk[2 * d + 1, g], preferred_element_type=F32))
                ld = -RATE_SCALE * rate * base[d : d + 1, lanes] + ex[:, lanes]
                bv[d, at, lanes] = jnp.sqrt(minus_expm1(2.0 * ld)) * admit * c.astype(F32)
                av[d, at, lanes] = jnp.exp(ld)

    one = jnp.ones((SEG, chan), F32)
    zero = jnp.zeros((SEG, chan), F32)

    def advance(i, carry):
        out = []
        for d in range(2):
            at = pl.ds(pl.multiple_of((i if d == 0 else seglen - 1 - i) * SEG, SEG), SEG)
            a, b = av[d, at, :], bv[d, at, :]
            cum = carry[2 * d] * a
            state = a * carry[2 * d + 1] + b
            av[d, at, :] = cum
            bv[d, at, :] = state
            out += [cum, state]
        return tuple(out)

    ends = lax.fori_loop(0, seglen, advance, (one, zero, one, zero))

    def run(d, entering):
        order = range(SEG) if d == 0 else range(SEG - 1, -1, -1)
        inside = [None] * SEG
        c = entering
        for s in order:
            inside[s] = c
            c = ends[2 * d][s : s + 1] * c + ends[2 * d + 1][s : s + 1]
        return jnp.concatenate(inside, axis=0), c

    for d in range(2):
        prod = ends[2 * d][0:1]
        for s in range(1, SEG):
            prod = prod * ends[2 * d][s : s + 1]
        msg[2 * d : 2 * d + 1, :] = prod
        msg[2 * d + 1 : 2 * d + 2, :] = run(d, jnp.zeros((1, chan), F32))[1]
    msg[4:8, :] = jnp.zeros((4, chan), F32)
    sent = []
    for k in range(1, n_sp):
        to = lax.rem(sp + k, n_sp)
        c = rcopy(msg, totals.at[k], tsend.at[k], trecv.at[k], sp=to)
        c.start()
        sent.append(c)
    for c in sent:
        c.wait()
    carries = []
    zrow = jnp.zeros((1, chan), F32)
    c0, c1 = zrow, zrow
    for k in range(n_sp - 1, 0, -1):
        t = totals[k]
        c0 = jnp.where(k <= sp, t[0:1] * c0 + t[1:2], c0)
    for k in range(1, n_sp):
        t = totals[k]
        c1 = jnp.where(k > sp, t[2:3] * c1 + t[3:4], c1)
    for d, c in ((0, c0), (1, c1)):
        inside = run(d, c)[0]
        carries.append(jnp.concatenate([inside, inside], axis=0))

    @pl.loop(0, rows // 16)
    def _(r):
        at = pl.ds(pl.multiple_of(r * 16, 16), 16)
        total = bv[0, at, :] + av[0, at, :] * carries[0]
        total = total + (bv[1, at, :] + av[1, at, :] * carries[1])
        mixedp[at, :] = (total * jax.nn.gelu(gperm[at, :].astype(F32))).astype(BF16)

    mixed[tp] = jnp.dot(perm[...], mixedp[...], preferred_element_type=F32).astype(BF16)

    half = rows // 2

    def mixed_slot(owner, part):
        return mixed.at[owner] if part is None else mixed.at[owner, pl.ds(part * half, half)]

    g = Gather(n_tp, mixed_slot, gsend, grecv)
    g.start()
    resid[...] = tokens[...].astype(F32)

    def project(owner):
        @pl.loop(0, rows // 128)
        def _(r):
            at = pl.ds(pl.multiple_of(r * 128, 128), 128)
            resid[at, :] += jnp.dot(mixed[owner, at, :], outw[owner], preferred_element_type=F32)

    load.wait()
    project(tp)
    g.forward()
    for owner in g.arrivals():
        project(owner)

    r2 = resid[...] * resid[...]
    sqown[...] = lax.dot_general(
        jnp.ones((8, cols), F32), r2, (((1,), (1,)), ((), ())),
        precision=EXACT, preferred_element_type=F32,
    )
    sent = []
    for k in range(1, n_tp):
        c = rcopy(sqown, squares.at[k], ssend.at[k], srecv.at[k], tp=lax.rem(tp + k, n_tp))
        c.start()
        sent.append(c)
    total = sqown[...]
    for k, c in enumerate(sent):
        c.wait()
        total = total + squares[k + 1]
    scale = lax.rsqrt(total / D + NORM_EPS)
    scale = lax.dot_general(
        scale, jnp.full((8, 128), 0.125, F32), (((0,), (0,)), ((), ())),
        precision=EXACT, preferred_element_type=F32,
    )[:, 0:1]
    normed[...] = (resid[...] * scale * gain[...]).astype(BF16)
    mine = pl.ds(pl.multiple_of(tp * cols, 128), cols)
    whole[:, mine] = normed[...]

    def normed_slot(owner, part):
        lanes = pl.ds(pl.multiple_of(owner * cols, 128), cols)
        at = pl.ds(0, rows) if part is None else pl.ds(part * half, half)
        return whole.at[at, lanes]

    h = Gather(n_tp, normed_slot, nsend, nrecv)
    h.start()
    g.drain()
    h.forward()
    for owner in h.arrivals():
        pass
    h.drain()


def front(n_sp, n_tp, rec, gate, conv_weight, dw, dn, iw, inn, base, extra, tokens, outw, gain):
    rows, chan = rec.shape
    heads, wide, narrow = dw.shape[1], dw.shape[2], dn.shape[2]
    cols = tokens.shape[1]
    per = 2 if heads % 2 == 0 else 1
    hw = wide + narrow
    gw = per * hw
    blocks = []
    for d in range(2):
        for w, n in ((dw, dn), (iw, inn)):
            w = w[d].reshape(heads // per, per, wide, wide)
            n = n[d].reshape(heads // per, per, narrow, narrow)
            block = 0
            for p in range(per):
                a = p * hw
                z = ((0, 0), (a, gw - a - wide), (a, gw - a - wide))
                block = block + jnp.pad(w[:, p], z)
                a += wide
                z = ((0, 0), (a, gw - a - narrow), (a, gw - a - narrow))
                block = block + jnp.pad(n[:, p], z)
            blocks.append(block)
    wblk = jnp.stack(blocks)
    seglen = rows // SEG
    ex = extra.reshape(2, SEG, seglen, 2 * heads).swapaxes(1, 2).reshape(2, rows, 2 * heads)
    c = np.arange(chan)
    which = (c % hw >= wide) * heads + c // hw
    spread = jnp.asarray((which[None, :] == np.arange(2 * heads)[:, None]).astype(np.float32))
    r = lax.broadcasted_iota(jnp.int32, (rows, rows), 0)
    q = lax.broadcasted_iota(jnp.int32, (rows, rows), 1)
    permt = ((r % SEG) * seglen + r // SEG == q).astype(BF16)
    perm = ((q % SEG) * seglen + q // SEG == r).astype(BF16)
    vm = pl.BlockSpec(memory_space=pltpu.VMEM)
    dma = pltpu.SemaphoreType.DMA
    return pl.pallas_call(
        functools.partial(front_kernel, n_sp, n_tp),
        name="front",
        out_shape=(
            jax.ShapeDtypeStruct((rows, cols), F32),
            jax.ShapeDtypeStruct((rows, n_tp * cols), BF16),
            jax.ShapeDtypeStruct((rows, cols), BF16),
        ),
        in_specs=[vm] * 10 + [pl.BlockSpec(memory_space=pl.ANY), vm],
        out_specs=(vm, vm, vm),
        scratch_shapes=[
            pltpu.VMEM((2, 16, chan), BF16),
            pltpu.VMEM((rows, chan), BF16),
            pltpu.VMEM((rows, chan), BF16),
            pltpu.VMEM((2, rows, chan), F32),
            pltpu.VMEM((2, rows, chan), F32),
            pltpu.VMEM((8, chan), F32),
            pltpu.VMEM((n_sp, 8, chan), F32),
            pltpu.VMEM((rows, chan), BF16),
            pltpu.VMEM((n_tp, rows, chan), BF16),
            pltpu.VMEM((n_tp, 8, rows), F32),
            pltpu.VMEM((8, rows), F32),
            dma((2,)), dma((2,)), dma((n_sp,)), dma((n_sp,)),
            *gather_sems(n_tp), dma((n_tp,)), dma((n_tp,)), *gather_sems(n_tp),
            pltpu.VMEM((n_tp, chan, cols), BF16), dma((1,)),
        ],
        compiler_params=pltpu.CompilerParams(
            collective_id=0, has_side_effects=True, vmem_limit_bytes=60 * 1024 * 1024
        ),
    )(
        rec, gate, conv_weight.astype(F32), wblk, base, ex, spread, perm, permt, tokens,
        outw.reshape(n_tp, chan, cols), gain.reshape(1, cols),
    )


def experts_kernel(
    n_sp, n_tp, cap,
    prow, pcol, weight, resid, whole, normed, hbm_sg, hbm_su, hbm_eg, hbm_eu, hbm_ed, hbm_sd,
    out,
    sg, su, eg, eu, ed, sd, outgoing, rows_in, hidden, answer, returned, shid, acc,
    wsem, dsend, drecv, asend, arecv, bsend, brecv, csend, crecv, rsend, rrecv,
):
    rows, cols = normed.shape
    ff = eg.shape[1]
    sp, tp = lax.axis_index("sp"), lax.axis_index("tp")
    count = 6 if n_tp == 4 else n_tp
    loads = []
    for i, (a, b) in enumerate(
        ((hbm_sg, sg), (hbm_su, su), (hbm_eg, eg), (hbm_eu, eu), (hbm_ed, ed), (hbm_sd, sd))
    ):
        c = pltpu.make_async_copy(a, b, wsem.at[i])
        c.start()
        loads.append(c)
    greet(n_sp, n_tp)

    slot = lax.broadcasted_iota(jnp.int32, (cap, rows), 0)
    mine = pl.ds(pl.multiple_of(tp * cols, 128), cols)
    fmine = pl.ds(pl.multiple_of(tp * ff, 128), ff)

    def dispatch(k):
        to = lax.rem(sp + k, n_sp)
        return rcopy(
            outgoing.at[to], rows_in.at[sp, :, mine], dsend.at[k], drecv.at[k], sp=to
        )

    def landed(k):
        src = lax.rem(sp - k + n_sp, n_sp)
        return rcopy(
            outgoing.at[src], rows_in.at[src, :, mine], dsend.at[k], drecv.at[k], sp=src
        )

    def reply(k):
        src = lax.rem(sp - k + n_sp, n_sp)
        return rcopy(answer.at[src], returned.at[sp], rsend.at[k], rrecv.at[k], sp=src)

    def replied(k):
        e = lax.rem(sp + k, n_sp)
        return rcopy(answer.at[e], returned.at[e], rsend.at[k], rrecv.at[k], sp=e)

    @pl.loop(0, n_sp)
    def _(k):
        e = lax.rem(sp + k, n_sp)
        hit = (prow[0:1, :] - e * cap == slot) | (prow[1:2, :] - e * cap == slot)
        picked = jnp.dot(
            hit.astype(F32).astype(BF16), normed[...], preferred_element_type=F32
        ).astype(BF16)

        @pl.when(k == 0)
        def _():
            rows_in[sp, :, mine] = picked

        @pl.when(k > 0)
        def _():
            outgoing[e] = picked
            dispatch(k).start()

    def gather(buffer, width, send, recv, k):
        src = lax.rem(sp - k + n_sp, n_sp)

        def place(owner, part):
            if part is None:
                return buffer.at[src, :, pl.ds(pl.multiple_of(owner * width, 128), width)]
            half = width // 2
            first = pl.multiple_of(owner * width + part * half, 128)
            return buffer.at[src, :, pl.ds(first, half)]

        return Gather(n_tp, place, send, recv, base=k * count)

    def rows_gather(k):
        return gather(rows_in, cols, asend, arecv, k)

    def hidden_gather(k):
        return gather(hidden, ff, bsend, brecv, k)

    def shared_place(owner, part):
        if part is None:
            return shid.at[:, pl.ds(pl.multiple_of(owner * ff, 128), ff)]
        half = ff // 2
        first = pl.multiple_of(owner * ff + part * half, 128)
        return shid.at[:, pl.ds(first, half)]

    shared = Gather(n_tp, shared_place, csend, crecv)
    rows_gather(0).start()
    loads[0].wait()
    loads[1].wait()

    @pl.loop(0, rows // 128)
    def _(r):
        at = pl.ds(pl.multiple_of(r * 128, 128), 128)
        x = whole[at, :]
        g = jnp.dot(x, sg[...], preferred_element_type=F32)
        u = jnp.dot(x, su[...], preferred_element_type=F32)
        shid[at, fmine] = (jax.nn.silu(g) * u).astype(BF16)

    shared.start()
    for c in loads[2:5]:
        c.wait()

    def combine(k):
        e = lax.rem(sp + k, n_sp)

        @pl.when(k > 0)
        def _():
            replied(k).wait_recv()

        lane = lax.broadcasted_iota(jnp.int32, (128, cap), 1)

        @pl.loop(0, rows // 128)
        def _(r):
            at = pl.ds(pl.multiple_of(r * 128, 128), 128)
            p0 = pcol[at, 0:1] - e * cap
            p1 = pcol[at, 1:2] - e * cap
            w = jnp.where((p0 >= 0) & (p0 < cap), weight[at, 0:1], 0.0) + jnp.where(
                (p1 >= 0) & (p1 < cap), weight[at, 1:2], 0.0
            )
            hit = ((p0 == lane) | (p1 == lane)).astype(F32).astype(BF16)
            acc[at, :] += w * jnp.dot(hit, returned[e], preferred_element_type=F32)

    @pl.loop(0, n_sp + 4)
    def _(step):
        @pl.when((step > 0) & (step < n_sp))
        def _():
            landed(step).wait_recv()
            rows_gather(step).start()

        @pl.when((step >= 1) & (step < n_sp + 1))
        def _():
            rows_gather(step - 1).forward()

        @pl.when((step >= 2) & (step < n_sp + 2))
        def _():
            k = step - 2
            src = lax.rem(sp - k + n_sp, n_sp)
            for _ in rows_gather(k).arrivals():
                pass
            x = rows_in[src]
            g = jnp.dot(x, eg[...], preferred_element_type=F32)
            u = jnp.dot(x, eu[...], preferred_element_type=F32)
            hidden[src, :, fmine] = (jax.nn.silu(g) * u).astype(BF16)
            hidden_gather(k).start()

        @pl.when(step == 1)
        def _():
            shared.forward()

        @pl.when(step == 4)
        def _():
            loads[5].wait()
            for _ in shared.arrivals():
                pass

            @pl.loop(0, rows // 128)
            def _(r):
                at = pl.ds(pl.multiple_of(r * 128, 128), 128)
                acc[at, :] = resid[at, :] + jnp.dot(
                    shid[at, :], sd[...], preferred_element_type=F32
                )

        @pl.when(step >= 6)
        def _():
            combine(step - 6)

        @pl.when((step >= 3) & (step < n_sp + 3))
        def _():
            hidden_gather(step - 3).forward()

        @pl.when(step >= 4)
        def _():
            k = step - 4
            src = lax.rem(sp - k + n_sp, n_sp)
            for _ in hidden_gather(k).arrivals():
                pass
            y = jnp.dot(hidden[src], ed[...], preferred_element_type=F32).astype(BF16)

            @pl.when(k == 0)
            def _():
                returned[sp] = y

            @pl.when(k > 0)
            def _():
                answer[src] = y
                reply(k).start()

    @pl.loop(n_sp - 2, n_sp)
    def _(k):
        combine(k)

    out[...] = acc[...].astype(BF16)
    shared.drain()

    @pl.loop(0, n_sp)
    def _(k):
        rows_gather(k).drain()
        hidden_gather(k).drain()

        @pl.when(k > 0)
        def _():
            dispatch(k).wait_send()
            reply(k).wait_send()


def experts(n_sp, n_tp, cap, placing, route_weight, resid, whole, normed, weights):
    rows, cols = normed.shape
    ff = weights[0].shape[1]
    vm = pl.BlockSpec(memory_space=pltpu.VMEM)
    hbm = pl.BlockSpec(memory_space=pl.ANY)
    dma = pltpu.SemaphoreType.DMA
    count = 6 if n_tp == 4 else n_tp
    return pl.pallas_call(
        functools.partial(experts_kernel, n_sp, n_tp, cap),
        name="experts",
        out_shape=jax.ShapeDtypeStruct((rows, cols), BF16),
        in_specs=[vm] * 6 + [hbm] * 6,
        out_specs=vm,
        scratch_shapes=[pltpu.VMEM(w.shape, BF16) for w in weights] + [
            pltpu.VMEM((n_sp, cap, cols), BF16),
            pltpu.VMEM((n_sp, cap, n_tp * cols), BF16),
            pltpu.VMEM((n_sp, cap, n_tp * ff), BF16),
            pltpu.VMEM((n_sp, cap, cols), BF16),
            pltpu.VMEM((n_sp, cap, cols), BF16),
            pltpu.VMEM((rows, n_tp * ff), BF16),
            pltpu.VMEM((rows, cols), F32),
            dma((6,)), dma((n_sp,)), dma((n_sp,)),
            dma((n_sp * count,)), dma((n_sp * count,)),
            dma((n_sp * count,)), dma((n_sp * count,)),
            *gather_sems(n_tp), dma((n_sp,)), dma((n_sp,)),
        ],
        compiler_params=pltpu.CompilerParams(
            collective_id=1, has_side_effects=True, vmem_limit_bytes=60 * 1024 * 1024
        ),
    )(placing.T, placing, route_weight, resid, whole, normed, *weights)


def shards(
    rec_input,
    gate_input,
    conv_weight,
    decay_wide,
    decay_narrow,
    input_wide,
    input_narrow,
    decay_base,
    decay_extra,
    tokens,
    out_weight,
    norm_gain,
    shared_gate,
    shared_up,
    shared_down,
    expert_gate,
    expert_up,
    expert_down,
    routes,
    route_weight,
):
    seq_rows = rec_input.shape[0]
    columns = out_weight.shape[1]
    resid, whole_rows, normed = front(
        lax.axis_size("sp"), lax.axis_size("tp"), rec_input, gate_input, conv_weight,
        decay_wide, decay_narrow, input_wide, input_narrow, decay_base, decay_extra,
        tokens, out_weight, norm_gain,
    )
    top_count = routes.shape[1]
    expert_count = lax.axis_size("sp")
    capacity = 3 * seq_rows * top_count // (2 * expert_count)
    flat_route = routes.reshape(-1)
    onehot = (flat_route[:, None] == jnp.arange(expert_count, dtype=jnp.int32)[None, :]).astype(
        jnp.int32
    )
    before = jnp.cumsum(onehot, axis=0) - onehot
    slot_ids = jnp.sum(before * onehot, axis=1)
    placing = (flat_route * capacity + slot_ids).reshape(seq_rows, top_count)
    return experts(
        expert_count, lax.axis_size("tp"), capacity, placing, route_weight, resid, whole_rows, normed,
        (shared_gate, shared_up, expert_gate[0], expert_up[0], expert_down[0], shared_down),
    )


def solution(mesh):
    placed = (
        P("sp", "tp"),
        P("sp", "tp"),
        P(None, "tp"),
        P(None, "tp", None, None),
        P(None, "tp", None, None),
        P(None, "tp", None, None),
        P(None, "tp", None, None),
        P(None, "tp"),
        P(None, "sp", None, "tp"),
        P("sp", "tp"),
        P(None, "tp"),
        P("tp"),
        P(None, "tp"),
        P(None, "tp"),
        P(None, "tp"),
        P("sp", None, "tp"),
        P("sp", None, "tp"),
        P("sp", None, "tp"),
        P("sp", None),
        P("sp", None),
    )
    return jax.shard_map(
        shards, mesh=mesh, in_specs=placed, out_specs=P("sp", "tp"), check_vma=False
    )
```

profile of v0, /device:TPU:0, one launch (start us, length us, event | category | flops | bytes accessed | tf_op | source)
XLA Modules:
  0.0 188.2 jit_solution(12927821856471493654)
XLA Ops:
  0.0 1.0 fusion.11
  1.1 1.0 fusion.12
  2.1 0.0 copy-done.1
  2.1 0.0 copy-done.2
  2.2 0.2 add_bitcast_fusion.2
  2.4 0.2 add_bitcast_fusion
  2.6 0.0 copy-start.3
  2.6 1.8 pad_maximum_fusion.wblk
  4.5 1.3 fusion.1
  5.7 0.0 copy-done.3
  5.7 0.1 reshape.33
  5.8 0.9 copy.75
  6.8 0.6 convert_element_type.38.convw
  7.4 67.8 %front.1 = (f32[384,512]{1,0:T(8,128)}, bf16[384,2048]{1,0:T(8,128)(2,1)}, bf16[384,512]{1,0:T(8,128)(2,1)}) custom-call(bf16[384,768]{1,0:T(8,128)(2,1)} %rec.1, bf16[384,768]{1,0:T(8,128)(2,1)} %gate.1, f32[4,768]{1,0:T(4,128)} %convert_element_type.38.convw, bf16[4,2,384,384]{3,2,1,0:T(8,128)(2,1)} %pad_maximum_fusion.wblk, f32[2,768]{1,0:T(2,128)} %base.1, ...), custom_call_target="tpu_custom_call" | custom-call | tf_op jit(solution)/shard_map/front/pallas_call | solution.py:318
  75.2 0.0 copy-start.6
  75.2 0.1 copy.54
  75.4 0.1 eq.38
  75.5 1.7 reduce-window.6
  77.3 0.1 slice.104
  77.3 0.1 copy.56
  77.5 0.2 reduce-window.9
  77.6 0.1 copy.57
  77.7 0.1 eq.34
  77.9 0.1 fusion.3
  78.0 0.2 reduce_sum.12
  78.1 0.1 copy.58
  78.3 0.0 copy-start
  78.3 0.7 copy.76.prow
  79.0 0.0 copy-done.6
  79.0 0.8 copy.77.weight
  79.9 106.6 %experts.1 = bf16[384,512]{1,0:T(8,128)(2,1)} custom-call(s32[2,384]{1,0:T(2,128)} %copy.76.prow, s32[384,2]{1,0:T(8,128)} %copy-done, f32[384,2]{1,0:T(8,128)} %copy.77.weight, f32[384,512]{1,0:T(8,128)} %get-tuple-element.8.resid, bf16[384,2048]{1,0:T(8,128)(2,1)} %get-tuple-element.9.whole, bf16[384,512]{1,0:T(8,128)(2,1)} %get-tuple-element.10.normed, ...), custom_call_target="tpu_custom_call" | custom-call | tf_op jit(solution)/shard_map/experts/pallas_call | solution.py:566
  186.4 1.8 copy.95
  (23 shorter events, 0.2 us)
Async XLA Ops:
  0.0 2.1 %copy-start.1 = (bf16[2,4,64,64]{3,2,1,0:T(8,128)(2,1)S(1)}, bf16[2,4,64,64]{3,2,1,0:T(8,128)(2,1)}, u32[]{:S(2)}) copy-start(bf16[2,4,64,64]{3,2,1,0:T(8,128)(2,1)} %param.25) | copy-start | bytes 196612
  0.0 2.1 %copy-start.2 = (bf16[2,4,64,64]{3,2,1,0:T(8,128)(2,1)S(1)}, bf16[2,4,64,64]{3,2,1,0:T(8,128)(2,1)}, u32[]{:S(2)}) copy-start(bf16[2,4,64,64]{3,2,1,0:T(8,128)(2,1)} %param.27) | copy-start | bytes 196612
  2.6 3.1 %copy-start.3 = (f32[2,384,2,4]{1,3,2,0:T(4,128)S(1)}, f32[2,384,2,4]{1,3,2,0:T(4,128)}, u32[]{:S(2)}) copy-start(f32[2,384,2,4]{1,3,2,0:T(4,128)} %param.29) | copy-start | bytes 73732
  4.4 2.3 %copy-start.5 = (bf16[4,768]{1,0:T(4,128)(2,1)S(1)}, bf16[4,768]{1,0:T(4,128)(2,1)}, u32[]{:S(2)}) copy-start(bf16[4,768]{1,0:T(4,128)(2,1)} %param.23) | copy-start | bytes 18436
  7.4 67.9 %copy-start.4 = (s32[384,2]{0,1:T(2,128)S(1)}, s32[384,2]{0,1:T(2,128)}, u32[]{:S(2)}) copy-start(s32[384,2]{0,1:T(2,128)} %param.39) | copy-start | bytes 9220
  75.2 3.8 %copy-start.6 = (f32[384,2]{0,1:T(2,128)S(1)}, f32[384,2]{0,1:T(2,128)}, u32[]{:S(2)}) copy-start(f32[384,2]{0,1:T(2,128)} %param.40) | copy-start | bytes 9220
  78.3 1.5 copy-start
where the time goes:
time: 188 us
  Pallas kernels  174 us (93%)
  local copies, waits for them, and re-layouts  7.47 us (4%)
  other arithmetic  6.06 us (3%)
    pallas_call x1, Pallas kernels, experts(): pl.pallas_call(functools.partial(experts_kernel, n_sp, n_tp, cap), name='...  107 us
    pallas_call x1, Pallas kernels, front(): pl.pallas_call(functools.partial(front_kernel, n_sp, n_tp), name='front',...  67.8 us

commit v1 on v0

v1 whole, which is shorter than its diff:
```python
import functools

import jax
import jax.numpy as jnp
import numpy as np
from jax import lax
from jax.experimental import pallas as pl
from jax.experimental.pallas import tpu as pltpu
from jax.sharding import PartitionSpec as P

MESH = pl.DeviceIdType.MESH
D = 2048
CONV = 4
NORM_EPS = 1e-06
RATE_SCALE = 8.0
SEG = 8
F32 = jnp.float32
BF16 = jnp.bfloat16
EXACT = lax.Precision.HIGHEST


def rcopy(src, dst, send, recv, **where):
    return pltpu.make_async_remote_copy(
        src_ref=src, dst_ref=dst, send_sem=send, recv_sem=recv, device_id=where, device_id_type=MESH
    )


def greet(n_sp, n_tp):
    sp, tp = lax.axis_index("sp"), lax.axis_index("tp")
    barrier = pltpu.get_barrier_semaphore()
    for k in range(1, n_sp):
        pl.semaphore_signal(
            barrier, inc=1, device_id={"sp": lax.rem(sp + k, n_sp)}, device_id_type=MESH
        )
    for k in range(1, n_tp):
        pl.semaphore_signal(
            barrier, inc=1, device_id={"tp": lax.rem(tp + k, n_tp)}, device_id_type=MESH
        )
    pl.semaphore_wait(barrier, n_sp + n_tp - 2)


def gather_sems(n_tp):
    count = 6 if n_tp == 4 else n_tp
    return [pltpu.SemaphoreType.DMA((count,)), pltpu.SemaphoreType.DMA((count,))]


class Gather:
    def __init__(self, n_tp, slot, send, recv, base=0):
        self.n, self.slot, self.send, self.recv, self.base = n_tp, slot, send, recv, base
        self.t = lax.axis_index("tp")
        if n_tp == 4:
            y, x = self.t // 2, lax.rem(self.t, 2)
            self.xn, self.yn, self.dg = y * 2 + 1 - x, (1 - y) * 2 + x, 3 - self.t

    def piece(self, owner, half, sem, to):
        ref = self.slot(owner, half)
        s = self.base + sem
        return rcopy(ref, ref, self.send.at[s], self.recv.at[s], tp=to)

    def start(self):
        if self.n == 4:
            self.piece(self.t, 0, 0, self.xn).start()
            self.piece(self.t, 1, 3, self.yn).start()
            self.piece(self.t, 1, 1, self.xn).start()
            self.piece(self.t, 0, 2, self.yn).start()
        else:
            for k in range(1, self.n):
                to = lax.rem(self.t + k, self.n)
                self.piece(self.t, None, k, to).start()

    def forward(self):
        if self.n == 4:
            self.piece(self.xn, 0, 0, self.xn).wait_recv()
            self.piece(self.xn, 0, 4, self.yn).start()
            self.piece(self.yn, 1, 3, self.yn).wait_recv()
            self.piece(self.yn, 1, 5, self.xn).start()

    def arrivals(self):
        if self.n == 4:
            self.piece(self.xn, 1, 1, self.xn).wait_recv()
            yield self.xn
            self.piece(self.yn, 0, 2, self.yn).wait_recv()
            yield self.yn
            self.piece(self.dg, 0, 4, self.yn).wait_recv()
            self.piece(self.dg, 1, 5, self.xn).wait_recv()
            yield self.dg
        else:
            for k in range(1, self.n):
                owner = lax.rem(self.t - k + self.n, self.n)
                self.piece(owner, None, k, owner).wait_recv()
                yield owner

    def drain(self):
        if self.n == 4:
            for s, half, owner in (
                (0, 0, self.t), (1, 1, self.t), (2, 0, self.t), (3, 1, self.t),
                (4, 0, self.xn), (5, 1, self.yn),
            ):
                self.piece(owner, half, s, self.xn).wait_send()
        else:
            for k in range(1, self.n):
                to = lax.rem(self.t + k, self.n)
                self.piece(self.t, None, k, to).wait_send()


def minus_expm1(y):
    series = 1.0 + y * (1 / 7.0)
    for d in (6.0, 5.0, 4.0, 3.0, 2.0):
        series = 1.0 + y * (1 / d) * series
    return jnp.where(y > -0.3, -y * series, 1.0 - jnp.exp(y))


class Order:
    def __init__(self, n_sp):
        sp = lax.axis_index("sp")
        chip = sp // 2
        self.core, self.low, self.high, self.n = sp % 2, chip % 2, chip // 2, n_sp // 4

    def at(self, p, sign):
        step = p // 4 + 1
        high = (self.high + (step if sign > 0 else 2 * self.n - step)) % self.n
        low = (self.low + 1 + p // 2) % 2
        return (high * 2 + low) * 2 + (self.core + 1 + p) % 2


class Square:
    def __init__(self):
        t, core = lax.axis_index("tp"), lax.axis_index("sp") % 2
        y, x = t // 2, t % 2
        xn, yn = y * 2 + 1 - x, (1 - y) * 2 + x
        flip = core == 1
        self.gather = jnp.where(flip, yn, xn)
        self.reduce = jnp.where(flip, xn, yn)
        self.place = jnp.where(flip, y, x)
        self.mine = (jnp.where(flip, x, 2 * y), jnp.where(flip, 2 + x, 2 * y + 1))
        self.theirs = (jnp.where(flip, 1 - x, 2 - 2 * y), jnp.where(flip, 3 - x, 3 - 2 * y))


def layer_kernel(
    n_sp, n_tp, cap, direct,
    rec, gate, convw, dw, dn, iw, inn, base, extra, spread, tokens, gain, routes, rweight,
    hbm_outw, hbm_sg, hbm_su, hbm_eg, hbm_eu, hbm_ed, hbm_sd,
    out,
    outw, sg, su, eg, eu, ed, sd, permt, perm, wblk, exs,
    halo, cperm, gperm, av, bv, msg, totals, mixedp, mixed, squares, sqown,
    resid, whole, normed, srow, scol, pos, wts, post, wtt,
    outgoing, outwide, rows_in, hidden, own, psend, precv, answer, returned, shid, spsend, sprecv,
    wsem, xsend, xrecv, hsend, hrecv, tsend, trecv, gsend, grecv, ssend, srecv, nsend, nrecv,
    dsend, drecv, asend, arecv, bsend, brecv, psem, prem, rsend, rrecv, csend, crecv, qsend, qrecv,
):
    two = n_tp == 4
    rows, chan = rec.shape
    heads, wide, narrow = dw.shape[1], dw.shape[2], dn.shape[2]
    groups, gw = wblk.shape[1], wblk.shape[2]
    cols = tokens.shape[1]
    ff = eg.shape[1]
    seglen = rows // SEG
    count = 6 if two else n_tp
    n_far = n_sp - direct
    sp, tp = lax.axis_index("sp"), lax.axis_index("tp")
    mine = pl.ds(pl.multiple_of(tp * cols, 128), cols)
    order = Order(n_sp)
    sq = Square() if two else None

    loads = []

    def load(a, b):
        c = pltpu.make_async_copy(a, b, wsem.at[len(loads)])
        c.start()
        loads.append(c)

    def band(i):
        return pl.ds(pl.multiple_of(i * ff, 128), ff)

    load(hbm_outw, outw)
    load(hbm_sg, sg)
    load(hbm_su, su)
    load(hbm_eg, eg)
    load(hbm_eu, eu)
    if two:
        for hbm, vmem in ((hbm_ed, ed), (hbm_sd, sd)):
            for j in range(2):
                load(hbm.at[band(sq.mine[j])], vmem.at[0, pl.ds(j * ff, ff)])
    else:
        load(hbm_ed, ed)
        load(hbm_sd, sd)
    greet(n_sp, n_tp)
    up, down = lax.rem(sp + 1, n_sp), lax.rem(sp + n_sp - 1, n_sp)
    low = rcopy(rec.at[pl.ds(rows - 16, 16)], halo.at[0], hsend.at[0], hrecv.at[0], sp=up)
    high = rcopy(rec.at[pl.ds(0, 16)], halo.at[1], hsend.at[1], hrecv.at[1], sp=down)
    low.start()
    high.start()
    swaps = []
    if two:
        for hbm, vmem in ((hbm_sd, sd), (hbm_ed, ed)):
            for j in range(2):
                i = len(swaps)
                c = rcopy(
                    hbm.at[band(sq.theirs[j])], vmem.at[1, pl.ds(j * ff, ff)],
                    xsend.at[i], xrecv.at[i], tp=sq.reduce,
                )
                c.start()
                swaps.append(c)

    r = lax.broadcasted_iota(jnp.int32, (rows, rows), 0)
    q = lax.broadcasted_iota(jnp.int32, (rows, rows), 1)
    permt[...] = jnp.where((r % SEG) * seglen + r // SEG == q, 1.0, 0.0).astype(BF16)
    perm[...] = jnp.where((q % SEG) * seglen + q // SEG == r, 1.0, 0.0).astype(BF16)
    wblk[...] = jnp.zeros_like(wblk)
    per = heads // groups
    for d in range(2):
        for k, (w, n) in enumerate(((dw, dn), (iw, inn))):
            for h in range(heads):
                a = (h % per) * (wide + narrow)
                b = a + wide
                wblk[2 * d + k, h // per, a:b, a:b] = w[d, h]
                wblk[2 * d + k, h // per, b : b + narrow, b : b + narrow] = n[d, h]
    for d in range(2):
        exs[d] = jnp.dot(
            permt[...].astype(F32), extra[d], precision=EXACT, preferred_element_type=F32
        )
    gperm[...] = jnp.dot(permt[...], gate[...], preferred_element_type=F32).astype(BF16)

    low.wait()
    high.wait()
    x = rec[...].astype(F32)
    taps = convw[...].astype(F32)
    lo = jnp.where(sp > 0, halo[0].astype(F32), 0.0)
    hi = jnp.where(sp < n_sp - 1, halo[1].astype(F32), 0.0)
    padded = jnp.concatenate([lo[14:16], x, hi[0:1]], axis=0)
    conv = padded[0:rows] * taps[0:1, :]
    for j in range(1, CONV):
        conv = conv + padded[j : j + rows] * taps[j : j + 1, :]
    cperm[...] = jnp.dot(
        permt[...], conv.astype(BF16), preferred_element_type=F32
    ).astype(BF16)

    step = 64

    @pl.loop(0, rows // step)
    def _(r):
        at = pl.ds(pl.multiple_of(r * step, step), step)
        for d in range(2):
            ex = jnp.dot(exs[d, at, :], spread[...], precision=EXACT, preferred_element_type=F32)
            for g in range(groups):
                lanes = slice(g * gw, (g + 1) * gw)
                c = cperm[at, lanes]
                rate = jax.nn.sigmoid(jnp.dot(c, wblk[2 * d, g], preferred_element_type=F32))
                admit = jax.nn.sigmoid(jnp.dot(c, wblk[2 * d + 1, g], preferred_element_type=F32))
                ld = -RATE_SCALE * rate * base[d : d + 1, lanes] + ex[:, lanes]
                bv[d, at, lanes] = jnp.sqrt(minus_expm1(2.0 * ld)) * admit * c.astype(F32)
                av[d, at, lanes] = jnp.exp(ld)

    one = jnp.ones((SEG, chan), F32)
    zero = jnp.zeros((SEG, chan), F32)

    def advance(i, carry):
        got = []
        for d in range(2):
            at = pl.ds(pl.multiple_of((i if d == 0 else seglen - 1 - i) * SEG, SEG), SEG)
            a, b = av[d, at, :], bv[d, at, :]
            cum = carry[2 * d] * a
            state = a * carry[2 * d + 1] + b
            av[d, at, :] = cum
            bv[d, at, :] = state
            got += [cum, state]
        return tuple(got)

    ends = lax.fori_loop(0, seglen, advance, (one, zero, one, zero))

    def run(d, entering):
        seq = range(SEG) if d == 0 else range(SEG - 1, -1, -1)
        inside = [None] * SEG
        c = entering
        for s in seq:
            inside[s] = c
            c = ends[2 * d][s : s + 1] * c + ends[2 * d + 1][s : s + 1]
        return jnp.concatenate(inside, axis=0), c

    for d in range(2):
        prod = ends[2 * d][0:1]
        for s in range(1, SEG):
            prod = prod * ends[2 * d][s : s + 1]
        msg[2 * d : 2 * d + 1, :] = prod
        msg[2 * d + 1 : 2 * d + 2, :] = run(d, jnp.zeros((1, chan), F32))[1]
    msg[4:8, :] = jnp.zeros((4, chan), F32)
    sent = []
    for k in range(1, n_sp):
        to = lax.rem(sp + k, n_sp)
        c = rcopy(msg, totals.at[k], tsend.at[k], trecv.at[k], sp=to)
        c.start()
        sent.append(c)

    part = lax.broadcasted_iota(jnp.int32, (n_sp, rows), 0)
    who = jnp.zeros((n_sp, rows), jnp.int32)
    for p in range(n_sp):
        who = jnp.where(part == p, order.at(p, 1), who)
    hit0 = jnp.where(routes[0:1, :] == who, 1.0, 0.0)
    hit1 = jnp.where(routes[1:2, :] == who, 1.0, 0.0)
    earlier = jnp.where(r < q, 1.0, 0.0).astype(BF16)
    slots = jnp.dot((hit0 + hit1).astype(BF16), earlier, preferred_element_type=F32)
    pos[...] = jnp.where(hit0 + hit1 > 0.0, slots, -1.0)
    wts[...] = hit0 * rweight[0:1, :] + hit1 * rweight[1:2, :]
    post[...] = jnp.transpose(pos[...])
    wtt[...] = jnp.transpose(wts[...])

    for c in sent:
        c.wait()
    carries = []
    zrow = jnp.zeros((1, chan), F32)
    c0, c1 = zrow, zrow
    for k in range(n_sp - 1, 0, -1):
        t = totals[k]
        c0 = jnp.where(k <= sp, t[0:1] * c0 + t[1:2], c0)
    for k in range(1, n_sp):
        t = totals[k]
        c1 = jnp.where(k > sp, t[2:3] * c1 + t[3:4], c1)
    for d, c in ((0, c0), (1, c1)):
        inside = run(d, c)[0]
        carries.append(jnp.concatenate([inside, inside], axis=0))

    @pl.loop(0, rows // 16)
    def _(r):
        at = pl.ds(pl.multiple_of(r * 16, 16), 16)
        total = bv[0, at, :] + av[0, at, :] * carries[0]
        total = total + (bv[1, at, :] + av[1, at, :] * carries[1])
        mixedp[at, :] = (total * jax.nn.gelu(gperm[at, :].astype(F32))).astype(BF16)

    mixed[tp] = jnp.dot(perm[...], mixedp[...], preferred_element_type=F32).astype(BF16)

    half = rows // 2

    def mixed_slot(owner, part):
        return mixed.at[owner] if part is None else mixed.at[owner, pl.ds(part * half, half)]

    g = Gather(n_tp, mixed_slot, gsend, grecv)
    g.start()
    resid[...] = tokens[...].astype(F32)

    def project(owner):
        @pl.loop(0, rows // 128)
        def _(r):
            at = pl.ds(pl.multiple_of(r * 128, 128), 128)
            resid[at, :] += jnp.dot(mixed[owner, at, :], outw[owner], preferred_element_type=F32)

    loads[0].wait()
    project(tp)
    g.forward()
    for owner in g.arrivals():
        project(owner)

    whole[:, mine] = (resid[...] * gain[...]).astype(BF16)

    def whole_slot(owner, part):
        lanes = pl.ds(pl.multiple_of(owner * cols, 128), cols)
        at = pl.ds(0, rows) if part is None else pl.ds(part * half, half)
        return whole.at[at, lanes]

    w = Gather(n_tp, whole_slot, nsend, nrecv)
    r2 = resid[...] * resid[...]
    sqown[...] = lax.dot_general(
        jnp.ones((8, cols), F32), r2, (((1,), (1,)), ((), ())),
        precision=EXACT, preferred_element_type=F32,
    )
    sent = []
    for k in range(1, n_tp):
        c = rcopy(sqown, squares.at[k], ssend.at[k], srecv.at[k], tp=lax.rem(tp + k, n_tp))
        c.start()
        sent.append(c)
    w.start()
    g.drain()
    total = sqown[...]
    for k, c in enumerate(sent):
        c.wait()
        total = total + squares[k + 1]
    srow[...] = lax.rsqrt(total / (n_tp * cols) + NORM_EPS)
    scol[...] = lax.dot_general(
        srow[...], jnp.full((8, 128), 0.125, F32), (((0,), (0,)), ((), ())),
        precision=EXACT, preferred_element_type=F32,
    )
    normed[...] = (resid[...] * scol[:, 0:1] * gain[...]).astype(BF16)

    slot = lax.broadcasted_iota(jnp.int32, (cap, rows), 0).astype(F32)

    def chosen(p):
        return jnp.where(pos[pl.ds(p, 1), :] == slot, 1.0, 0.0)

    def far_copy(p, sign):
        return rcopy(
            outgoing.at[p], rows_in.at[p, :, mine], dsend.at[p], drecv.at[p], sp=order.at(p, sign)
        )

    def near_copy(p, sign):
        return rcopy(
            outwide.at[p - n_far], rows_in.at[p], dsend.at[p], drecv.at[p], sp=order.at(p, sign)
        )

    def reply(p):
        return rcopy(answer.at[p], returned.at[p], rsend.at[p], rrecv.at[p], sp=order.at(p, -1))

    @pl.loop(0, n_far)
    def _(p):
        outgoing[p] = jnp.dot(
            chosen(p).astype(BF16), normed[...], preferred_element_type=F32
        ).astype(BF16)
        far_copy(p, 1).start()

    def rows_gather(p):
        def place(owner, part):
            if part is None:
                return rows_in.at[p, :, pl.ds(pl.multiple_of(owner * cols, 128), cols)]
            first = pl.multiple_of(owner * cols + part * (cols // 2), 128)
            return rows_in.at[p, :, pl.ds(first, cols // 2)]

        return Gather(n_tp, place, asend, arecv, base=p * count)

    def begin_rows(p):
        far_copy(p, -1).wait_recv()
        rows_gather(p).start()

    lead = 2
    w.forward()
    for p in range(lead):
        begin_rows(p)
    for owner in w.arrivals():
        pass

    def wide_pick(p):
        hit = chosen(p)
        scale = jnp.sum(hit * srow[0:1, :], axis=1, keepdims=True)
        picked = jnp.dot(hit.astype(BF16), whole[...], preferred_element_type=F32)
        return (picked * scale).astype(BF16)

    @pl.loop(n_far, n_sp - 1)
    def _(p):
        outwide[p - n_far] = wide_pick(p)
        near_copy(p, 1).start()

    rows_in[n_sp - 1] = wide_pick(n_sp - 1)

    if two:
        here = pl.ds(pl.multiple_of(sq.place * ff, 128), ff)

        def give_hidden(p):
            ref = hidden.at[p, :, here]
            return rcopy(ref, ref, bsend.at[p], brecv.at[p], tp=sq.gather)

        def take_hidden(p):
            ref = hidden.at[p, :, pl.ds(pl.multiple_of((1 - sq.place) * ff, 128), ff)]
            return rcopy(ref, ref, bsend.at[p], brecv.at[p], tp=sq.gather)

        def give_part(p):
            return rcopy(psend.at[p], precv.at[p], psem.at[p], prem.at[p], tp=sq.reduce)

        sref = shid.at[:, here]
        sgive = rcopy(sref, sref, csend.at[0], crecv.at[0], tp=sq.gather)
        sref = shid.at[:, pl.ds(pl.multiple_of((1 - sq.place) * ff, 128), ff)]
        stake = rcopy(sref, sref, csend.at[0], crecv.at[0], tp=sq.gather)
        sgivep = rcopy(spsend, sprecv, qsend.at[0], qrecv.at[0], tp=sq.reduce)
    else:
        here = band(tp)

        def shared_place(owner, part):
            return shid.at[:, band(owner)]

        shared = Gather(n_tp, shared_place, csend, crecv)

        def hidden_gather(p):
            def place(owner, part):
                return hidden.at[p, :, band(owner)]

            return Gather(n_tp, place, bsend, brecv, base=p * count)

    loads[1].wait()
    loads[2].wait()

    @pl.loop(0, rows // 128)
    def _(r):
        at = pl.ds(pl.multiple_of(r * 128, 128), 128)
        x = whole[at, :]
        s = scol[at, 0:1]
        g = jnp.dot(x, sg[...], preferred_element_type=F32) * s
        u = jnp.dot(x, su[...], preferred_element_type=F32) * s
        shid[at, here] = (jax.nn.silu(g) * u).astype(BF16)

    if two:
        sgive.start()
    else:
        shared.start()
    w.drain()
    for c in loads[3:]:
        c.wait()
    for c in swaps:
        c.wait()

    def answer_with(p, y):
        @pl.when(p == n_sp - 1)
        def _():
            returned[p] = y

        @pl.when(p < n_sp - 1)
        def _():
            answer[p] = y
            reply(p).start()

    def combine(p):
        @pl.when(p < n_sp - 1)
        def _():
            reply(p).wait_recv()

        lane = lax.broadcasted_iota(jnp.int32, (128, cap), 1).astype(F32)
        which = lax.broadcasted_iota(jnp.int32, (128, n_sp), 1) == p

        @pl.loop(0, rows // 128)
        def _(r):
            at = pl.ds(pl.multiple_of(r * 128, 128), 128)
            where = jnp.sum(jnp.where(which, post[at, :], 0.0), axis=1, keepdims=True)
            weight = jnp.sum(jnp.where(which, wtt[at, :], 0.0), axis=1, keepdims=True)
            hit = jnp.where(where == lane, 1.0, 0.0).astype(BF16)
            resid[at, :] += weight * jnp.dot(hit, returned[p], preferred_element_type=F32)

    back = 4

    @pl.loop(0, n_sp + 3)
    def _(s):
        @pl.when(s + lead < n_far)
        def _():
            begin_rows(s + lead)

        @pl.when(s == 0)
        def _():
            rows_gather(0).forward()

        @pl.when(s + 1 < n_far)
        def _():
            rows_gather(s + 1).forward()

        @pl.when(s < n_sp)
        def _():
            @pl.when(s < n_far)
            def _():
                for _ in rows_gather(s).arrivals():
                    pass

            @pl.when((s >= n_far) & (s < n_sp - 1))
            def _():
                near_copy(s, -1).wait_recv()

            x = rows_in[s]
            g = jnp.dot(x, eg[...], preferred_element_type=F32)
            u = jnp.dot(x, eu[...], preferred_element_type=F32)
            hidden[s, :, here] = (jax.nn.silu(g) * u).astype(BF16)
            if two:
                give_hidden(s).start()
            else:
                hidden_gather(s).start()

        if two:
            @pl.when(s == 1)
            def _():
                stake.wait_recv()

                @pl.loop(0, rows // 128)
                def _(r):
                    at = pl.ds(pl.multiple_of(r * 128, 128), 128)
                    h = shid[at, :]
                    resid[at, :] += jnp.dot(h, sd[0], preferred_element_type=F32)
                    spsend[at, :] = jnp.dot(h, sd[1], preferred_element_type=F32).astype(BF16)

                sgivep.start()

            @pl.when(s == 3)
            def _():
                sgivep.wait_recv()
                resid[...] += sprecv[...].astype(F32)
        else:
            @pl.when(s == 1)
            def _():
                for _ in shared.arrivals():
                    pass

                @pl.loop(0, rows // 128)
                def _(r):
                    at = pl.ds(pl.multiple_of(r * 128, 128), 128)
                    resid[at, :] += jnp.dot(shid[at, :], sd[...], preferred_element_type=F32)

        @pl.when((s >= 1) & (s < n_sp + 1))
        def _():
            p = s - 1
            if two:
                take_hidden(p).wait_recv()
                h = hidden[p]
                psend[p] = jnp.dot(h, ed[1], preferred_element_type=F32).astype(BF16)
                give_part(p).start()
                own[p] = jnp.dot(h, ed[0], preferred_element_type=F32)
            else:
                for _ in hidden_gather(p).arrivals():
                    pass
                answer_with(
                    p, jnp.dot(hidden[p], ed[...], preferred_element_type=F32).astype(BF16)
                )

        if two:
            @pl.when((s >= 2) & (s < n_sp + 2))
            def _():
                p = s - 2
                give_part(p).wait_recv()
                answer_with(p, (own[p] + precv[p].astype(F32)).astype(BF16))

        @pl.when(s >= back)
        def _():
            combine(s - back)

    @pl.loop(n_sp + 3 - back, n_sp)
    def _(p):
        combine(p)

    out[...] = resid[...].astype(BF16)

    if two:
        sgive.wait_send()
        sgivep.wait_send()
    else:
        shared.drain()

    @pl.loop(0, n_sp)
    def _(p):
        if two:
            give_hidden(p).wait_send()
            give_part(p).wait_send()
        else:
            hidden_gather(p).drain()

        @pl.when(p < n_far)
        def _():
            rows_gather(p).drain()
            far_copy(p, 1).wait_send()

        @pl.when((p >= n_far) & (p < n_sp - 1))
        def _():
            near_copy(p, 1).wait_send()

        @pl.when(p < n_sp - 1)
        def _():
            reply(p).wait_send()


def shards(
    rec_input,
    gate_input,
    conv_weight,
    decay_wide,
    decay_narrow,
    input_wide,
    input_narrow,
    decay_base,
    decay_extra,
    tokens,
    out_weight,
    norm_gain,
    shared_gate,
    shared_up,
    shared_down,
    expert_gate,
    expert_up,
    expert_down,
    routes,
    route_weight,
):
    n_sp, n_tp = lax.axis_size("sp"), lax.axis_size("tp")
    rows, chan = rec_input.shape
    heads, wide, narrow = decay_wide.shape[1], decay_wide.shape[2], decay_narrow.shape[2]
    cols = tokens.shape[1]
    ff = shared_gate.shape[1]
    per = 2 if heads % 2 == 0 else 1
    hw = wide + narrow
    groups, gw = heads // per, per * hw
    cap = 3 * rows * routes.shape[1] // (2 * n_sp)
    direct = 4
    n_far = n_sp - direct
    two = n_tp == 4
    ex = decay_extra.reshape(2, rows, 2 * heads)
    c = np.arange(chan)
    which = (c % hw >= wide) * heads + c // hw
    spread = jnp.asarray((which[None, :] == np.arange(2 * heads)[:, None]).astype(np.float32))
    vm = pl.BlockSpec(memory_space=pltpu.VMEM)
    hbm = pl.BlockSpec(memory_space=pl.ANY)
    sem = pltpu.SemaphoreType.DMA
    count = 6 if two else n_tp
    down = (2, 2 * ff, cols) if two else (n_tp * ff, cols)
    hid = 2 * ff if two else n_tp * ff
    V = pltpu.VMEM
    pairs = [(4,), (2,), (n_sp,), (count,), (n_tp,), (count,), (n_sp,), (n_sp * count,)]
    pairs += [(n_sp,) if two else (n_sp * count,), (n_sp,), (n_sp,), (1,) if two else (count,), (1,)]
    return pl.pallas_call(
        functools.partial(layer_kernel, n_sp, n_tp, cap, direct),
        name="layer",
        out_shape=jax.ShapeDtypeStruct((rows, cols), BF16),
        in_specs=[vm] * 14 + [hbm] * 7,
        out_specs=vm,
        scratch_shapes=[
            V((n_tp, chan, cols), BF16), V(shared_gate.shape, BF16), V(shared_up.shape, BF16),
            V(expert_gate.shape[1:], BF16), V(expert_up.shape[1:], BF16), V(down, BF16), V(down, BF16),
            V((rows, rows), BF16), V((rows, rows), BF16), V((4, groups, gw, gw), BF16),
            V((2, rows, 2 * heads), F32),
            V((2, 16, chan), BF16), V((rows, chan), BF16), V((rows, chan), BF16),
            V((2, rows, chan), F32), V((2, rows, chan), F32),
            V((8, chan), F32), V((n_sp, 8, chan), F32), V((rows, chan), BF16),
            V((n_tp, rows, chan), BF16), V((n_tp, 8, rows), F32), V((8, rows), F32),
            V((rows, cols), F32), V((rows, n_tp * cols), BF16), V((rows, cols), BF16),
            V((8, rows), F32), V((rows, 128), F32),
            V((n_sp, rows), F32), V((n_sp, rows), F32), V((rows, n_sp), F32), V((rows, n_sp), F32),
            V((n_far, cap, cols), BF16), V((direct - 1, cap, n_tp * cols), BF16),
            V((n_sp, cap, n_tp * cols), BF16), V((n_sp, cap, hid), BF16),
            V((n_sp, cap, cols), F32), V((n_sp, cap, cols), BF16), V((n_sp, cap, cols), BF16),
            V((n_sp, cap, cols), BF16), V((n_sp, cap, cols), BF16),
            V((rows, hid), BF16), V((rows, cols), BF16), V((rows, cols), BF16),
            sem((9,)),
        ] + [sem(s) for s in pairs for _ in range(2)],
        compiler_params=pltpu.CompilerParams(
            collective_id=0, has_side_effects=True, vmem_limit_bytes=60 * 1024 * 1024
        ),
    )(
        rec_input, gate_input, conv_weight, decay_wide, decay_narrow, input_wide, input_narrow,
        decay_base, ex, spread, tokens, norm_gain.reshape(1, cols), routes.T, route_weight.T,
        out_weight.reshape(n_tp, chan, cols), shared_gate, shared_up, expert_gate[0], expert_up[0],
        expert_down[0], shared_down,
    )


def solution(mesh):
    placed = (
        P("sp", "tp"),
        P("sp", "tp"),
        P(None, "tp"),
        P(None, "tp", None, None),
        P(None, "tp", None, None),
        P(None, "tp", None, None),
        P(None, "tp", None, None),
        P(None, "tp"),
        P(None, "sp", None, "tp"),
        P("sp", "tp"),
        P(None, "tp"),
        P("tp"),
        P(None, "tp"),
        P(None, "tp"),
        P(None, "tp"),
        P("sp", None, "tp"),
        P("sp", None, "tp"),
        P("sp", None, "tp"),
        P("sp", None),
        P("sp", None),
    )
    return jax.shard_map(
        shards, mesh=mesh, in_specs=placed, out_specs=P("sp", "tp"), check_vma=False
    )
```

time: 188 us -> 150 us (0.80)
  Pallas kernels: 174 us -> 146 us
  other arithmetic: 6.06 us -> 0 us
  local copies, waits for them, and re-layouts: 7.47 us -> 3.44 us
    pallas_call x2 -> x1, Pallas kernels: 174 us -> 146 us  [shards(): pl.pallas_call(functools.partial(layer_kernel, n_sp, n_tp, cap, direct),...]
    another operation x5 -> x0, other arithmetic: 4.07 us -> none  [the longest x3 2.2 us: front(): wblk = jnp.stack(blocks)]
    slice x6 -> x0, local copies, waits for them, and re-layouts: 2.25 us -> none  [the longest x2 2.02 us: front(): w = w[d].reshape(heads // per, per, wide, wide)]
where the time goes in v1:
time: 150 us
  Pallas kernels  146 us (97%)
  local copies, waits for them, and re-layouts  3.44 us (2%)
    pallas_call x1, Pallas kernels, shards(): pl.pallas_call(functools.partial(layer_kernel, n_sp, n_tp, cap, direct),...  146 us

profile of v1, /device:TPU:0, one launch (start us, length us, event | category | flops | bytes accessed | tf_op | source)
XLA Modules:
  0.0 149.7 jit_solution(14243849433939858126)
XLA Ops:
  0.0 0.8 copy.23
  0.8 0.9 copy.24.extra
  1.7 146.3 %layer.1 = bf16[384,512]{1,0:T(8,128)(2,1)} custom-call(bf16[384,768]{1,0:T(8,128)(2,1)} %rec.1, bf16[384,768]{1,0:T(8,128)(2,1)} %gate.1, bf16[4,768]{1,0:T(4,128)(2,1)} %convw.1, bf16[2,4,128,128]{3,2,1,0:T(8,128)(2,1)} %dw.1, bf16[2,4,64,64]{3,2,1,0:T(8,128)(2,1)} %dn.1, bf16[2,4,128,128]{3,2,1,0:T(8,128)(2,1)} %iw.1, bf16[2,4,64,64]{3,2,1,0:T(8,128)(2,1)} %inn.1, ...), custom_call_target="tpu_custom_call" | custom-call | tf_op jit(solution)/shard_map/layer/pallas_call | solution.py:695
  147.9 1.8 %copy.26 = bf16[384,512]{1,0:T(8,128)(2,1)} copy(bf16[384,512]{1,0:T(8,128)(2,1)} %layer.1) | data formatting | bytes 786432

commit v2 on v1

--- a/solution.py
+++ b/solution.py
@@ -2,7 +2,6 @@
 
 import jax
 import jax.numpy as jnp
-import numpy as np
 from jax import lax
 from jax.experimental import pallas as pl
 from jax.experimental.pallas import tpu as pltpu
@@ -25,7 +24,7 @@
     )
 
 
-def greet(n_sp, n_tp):
+def hello(n_sp, n_tp):
     sp, tp = lax.axis_index("sp"), lax.axis_index("tp")
     barrier = pltpu.get_barrier_semaphore()
     for k in range(1, n_sp):
@@ -36,7 +35,10 @@
         pl.semaphore_signal(
             barrier, inc=1, device_id={"tp": lax.rem(tp + k, n_tp)}, device_id_type=MESH
         )
-    pl.semaphore_wait(barrier, n_sp + n_tp - 2)
+
+
+def met(n_sp, n_tp):
+    pl.semaphore_wait(pltpu.get_barrier_semaphore(), n_sp + n_tp - 2)
 
 
 def gather_sems(n_tp):
@@ -103,11 +105,8 @@
                 self.piece(self.t, None, k, to).wait_send()
 
 
-def minus_expm1(y):
-    series = 1.0 + y * (1 / 7.0)
-    for d in (6.0, 5.0, 4.0, 3.0, 2.0):
-        series = 1.0 + y * (1 / d) * series
-    return jnp.where(y > -0.3, -y * series, 1.0 - jnp.exp(y))
+def logistic(x):
+    return 0.5 * jnp.tanh(0.5 * x) + 0.5
 
 
 class Order:
@@ -138,15 +137,16 @@
 
 def layer_kernel(
     n_sp, n_tp, cap, direct,
-    rec, gate, convw, dw, dn, iw, inn, base, extra, spread, tokens, gain, routes, rweight,
-    hbm_outw, hbm_sg, hbm_su, hbm_eg, hbm_eu, hbm_ed, hbm_sd,
+    h_rec, h_gate, h_convw, h_dw, h_dn, h_iw, h_inn, h_base, h_extra, h_tokens, h_gain, h_routes,
+    h_rweight, hbm_outw, hbm_sg, hbm_su, hbm_eg, hbm_eu, hbm_ed, hbm_sd,
     out,
+    rec, gate, convw, dw, dn, iw, inn, base, extra, tokens, gain, routes, rweight,
     outw, sg, su, eg, eu, ed, sd, permt, perm, wblk, exs,
     halo, cperm, gperm, av, bv, msg, totals, mixedp, mixed, squares, sqown,
-    resid, whole, normed, srow, scol, pos, wts, post, wtt,
-    outgoing, outwide, rows_in, hidden, own, psend, precv, answer, returned, shid, spsend, sprecv,
-    wsem, xsend, xrecv, hsend, hrecv, tsend, trecv, gsend, grecv, ssend, srecv, nsend, nrecv,
-    dsend, drecv, asend, arecv, bsend, brecv, psem, prem, rsend, rrecv, csend, crecv, qsend, qrecv,
+    resid, whole, srow, scol, smsg, sgot, pos, wts, post, wtt,
+    outgoing, outwide, rows_in, hidden, own, psend, precv, answer, returned, shid,
+    isem, wsem, xsend, xrecv, hsend, hrecv, tsend, trecv, gsend, grecv, ssend, srecv, nsend, nrecv,
+    dsend, drecv, asend, arecv, bsend, brecv, psem, prem, rsend, rrecv, csend, crecv, lsend, lrecv,
 ):
     two = n_tp == 4
     rows, chan = rec.shape
@@ -172,19 +172,29 @@
     def band(i):
         return pl.ds(pl.multiple_of(i * ff, 128), ff)
 
+    ready = []
+    for i, (a, b) in enumerate((
+        (h_rec, rec), (h_convw, convw), (h_extra, extra), (h_gate, gate), (h_dw, dw), (h_dn, dn),
+        (h_iw, iw), (h_inn, inn), (h_base, base), (h_tokens, tokens), (h_gain, gain),
+        (h_routes, routes), (h_rweight, rweight),
+    )):
+        c = pltpu.make_async_copy(a, b, isem.at[i])
+        c.start()
+        ready.append(c)
+    hello(n_sp, n_tp)
     load(hbm_outw, outw)
     load(hbm_sg, sg)
     load(hbm_su, su)
     load(hbm_eg, eg)
     load(hbm_eu, eu)
+    load(hbm_sd, sd)
     if two:
-        for hbm, vmem in ((hbm_ed, ed), (hbm_sd, sd)):
-            for j in range(2):
-                load(hbm.at[band(sq.mine[j])], vmem.at[0, pl.ds(j * ff, ff)])
+        for j in range(2):
+            load(hbm_ed.at[band(sq.mine[j])], ed.at[0, pl.ds(j * ff, ff)])
     else:
         load(hbm_ed, ed)
-        load(hbm_sd, sd)
-    greet(n_sp, n_tp)
+    ready[0].wait()
+    met(n_sp, n_tp)
     up, down = lax.rem(sp + 1, n_sp), lax.rem(sp + n_sp - 1, n_sp)
     low = rcopy(rec.at[pl.ds(rows - 16, 16)], halo.at[0], hsend.at[0], hrecv.at[0], sp=up)
     high = rcopy(rec.at[pl.ds(0, 16)], halo.at[1], hsend.at[1], hrecv.at[1], sp=down)
@@ -192,15 +202,15 @@
     high.start()
     swaps = []
     if two:
-        for hbm, vmem in ((hbm_sd, sd), (hbm_ed, ed)):
-            for j in range(2):
-                i = len(swaps)
-                c = rcopy(
-                    hbm.at[band(sq.theirs[j])], vmem.at[1, pl.ds(j * ff, ff)],
-                    xsend.at[i], xrecv.at[i], tp=sq.reduce,
-                )
-                c.start()
-                swaps.append(c)
+        for j in range(2):
+            c = rcopy(
+                hbm_ed.at[band(sq.theirs[j])], ed.at[1, pl.ds(j * ff, ff)],
+                xsend.at[j], xrecv.at[j], tp=sq.reduce,
+            )
+            c.start()
+            swaps.append(c)
+    for c in ready[1:]:
+        c.wait()
 
     r = lax.broadcasted_iota(jnp.int32, (rows, rows), 0)
     q = lax.broadcasted_iota(jnp.int32, (rows, rows), 1)
@@ -216,9 +226,13 @@
                 wblk[2 * d + k, h // per, a:b, a:b] = w[d, h]
                 wblk[2 * d + k, h // per, b : b + narrow, b : b + narrow] = n[d, h]
     for d in range(2):
+        left, terms = extra[d], []
+        for _ in range(3):
+            terms.append(left.astype(BF16))
+            left = left - terms[-1].astype(F32)
         exs[d] = jnp.dot(
-            permt[...].astype(F32), extra[d], precision=EXACT, preferred_element_type=F32
-        )
+            permt[...], jnp.concatenate(terms, axis=1), preferred_element_type=F32
+        ).astype(BF16)
     gperm[...] = jnp.dot(permt[...], gate[...], preferred_element_type=F32).astype(BF16)
 
     low.wait()
@@ -235,21 +249,27 @@
         permt[...], conv.astype(BF16), preferred_element_type=F32
     ).astype(BF16)
 
-    step = 64
+    hw = wide + narrow
+    ch = lax.broadcasted_iota(jnp.int32, (6 * heads, chan), 1)
+    head, within = ch // hw, ch % hw
+    term = lax.broadcasted_iota(jnp.int32, (6 * heads, chan), 0) % (2 * heads)
+    spread = jnp.where(term == jnp.where(within >= wide, heads, 0) + head, 1.0, 0.0).astype(BF16)
+    step = rows // 2
 
     @pl.loop(0, rows // step)
     def _(r):
         at = pl.ds(pl.multiple_of(r * step, step), step)
         for d in range(2):
-            ex = jnp.dot(exs[d, at, :], spread[...], precision=EXACT, preferred_element_type=F32)
+            ex = jnp.dot(exs[d, at, :], spread, preferred_element_type=F32)
             for g in range(groups):
                 lanes = slice(g * gw, (g + 1) * gw)
                 c = cperm[at, lanes]
-                rate = jax.nn.sigmoid(jnp.dot(c, wblk[2 * d, g], preferred_element_type=F32))
-                admit = jax.nn.sigmoid(jnp.dot(c, wblk[2 * d + 1, g], preferred_element_type=F32))
-                ld = -RATE_SCALE * rate * base[d : d + 1, lanes] + ex[:, lanes]
-                bv[d, at, lanes] = jnp.sqrt(minus_expm1(2.0 * ld)) * admit * c.astype(F32)
-                av[d, at, lanes] = jnp.exp(ld)
+                rate = logistic(jnp.dot(c, wblk[2 * d, g], preferred_element_type=F32))
+                admit = logistic(jnp.dot(c, wblk[2 * d + 1, g], preferred_element_type=F32))
+                ld = jnp.minimum(ex[:, lanes] - rate * (RATE_SCALE * base[d : d + 1, lanes]), 0.0)
+                a = jnp.exp(ld)
+                bv[d, at, lanes] = jnp.sqrt(jnp.tanh(-ld) * (1.0 + a * a)) * admit * c.astype(F32)
+                av[d, at, lanes] = a
 
     one = jnp.ones((SEG, chan), F32)
     zero = jnp.zeros((SEG, chan), F32)
@@ -281,13 +301,14 @@
         prod = ends[2 * d][0:1]
         for s in range(1, SEG):
             prod = prod * ends[2 * d][s : s + 1]
-        msg[2 * d : 2 * d + 1, :] = prod
-        msg[2 * d + 1 : 2 * d + 2, :] = run(d, jnp.zeros((1, chan), F32))[1]
-    msg[4:8, :] = jnp.zeros((4, chan), F32)
+        msg[d, 0:1, :] = prod
+        msg[d, 1:2, :] = run(d, jnp.zeros((1, chan), F32))[1]
     sent = []
     for k in range(1, n_sp):
         to = lax.rem(sp + k, n_sp)
-        c = rcopy(msg, totals.at[k], tsend.at[k], trecv.at[k], sp=to)
+        c = rcopy(
+            msg.at[jnp.where(to > sp, 0, 1)], totals.at[k], tsend.at[k], trecv.at[k], sp=to
+        )
         c.start()
         sent.append(c)
 
@@ -314,7 +335,7 @@
         c0 = jnp.where(k <= sp, t[0:1] * c0 + t[1:2], c0)
     for k in range(1, n_sp):
         t = totals[k]
-        c1 = jnp.where(k > sp, t[2:3] * c1 + t[3:4], c1)
+        c1 = jnp.where(k > sp, t[0:1] * c1 + t[1:2], c1)
     for d, c in ((0, c0), (1, c1)):
         inside = run(d, c)[0]
         carries.append(jnp.concatenate([inside, inside], axis=0))
@@ -328,35 +349,46 @@
 
     mixed[tp] = jnp.dot(perm[...], mixedp[...], preferred_element_type=F32).astype(BF16)
 
-    half = rows // 2
-
-    def mixed_slot(owner, part):
-        return mixed.at[owner] if part is None else mixed.at[owner, pl.ds(part * half, half)]
-
-    g = Gather(n_tp, mixed_slot, gsend, grecv)
-    g.start()
+    half, quarter = rows // 2, rows // 4
+
+    def rows_of(i, part):
+        return pl.ds(i * half, half) if part is None else pl.ds(i * half + part * quarter, quarter)
+
+    def mixed_slot(i):
+        return lambda owner, part: mixed.at[owner, rows_of(i, part)]
+
+    def whole_slot(i):
+        return lambda owner, part: whole.at[
+            rows_of(i, part), pl.ds(pl.multiple_of(owner * cols, 128), cols)
+        ]
+
+    g = [Gather(n_tp, mixed_slot(i), gsend, grecv, base=i * count) for i in range(2)]
+    w = [Gather(n_tp, whole_slot(i), nsend, nrecv, base=i * count) for i in range(2)]
+
+    def project(owner, i):
+        at = pl.ds(i * half, half)
+        resid[at, :] += jnp.dot(mixed[owner, at, :], outw[owner], preferred_element_type=F32)
+
+    def publish(i):
+        at = pl.ds(i * half, half)
+        whole[at, mine] = (resid[at, :] * gain[...]).astype(BF16)
+
+    g[0].start()
     resid[...] = tokens[...].astype(F32)
-
-    def project(owner):
-        @pl.loop(0, rows // 128)
-        def _(r):
-            at = pl.ds(pl.multiple_of(r * 128, 128), 128)
-            resid[at, :] += jnp.dot(mixed[owner, at, :], outw[owner], preferred_element_type=F32)
-
     loads[0].wait()
-    project(tp)
-    g.forward()
-    for owner in g.arrivals():
-        project(owner)
-
-    whole[:, mine] = (resid[...] * gain[...]).astype(BF16)
-
-    def whole_slot(owner, part):
-        lanes = pl.ds(pl.multiple_of(owner * cols, 128), cols)
-        at = pl.ds(0, rows) if part is None else pl.ds(part * half, half)
-        return whole.at[at, lanes]
-
-    w = Gather(n_tp, whole_slot, nsend, nrecv)
+    project(tp, 0)
+    project(tp, 1)
+    g[0].forward()
+    g[1].start()
+    for owner in g[0].arrivals():
+        project(owner, 0)
+    publish(0)
+    g[1].forward()
+    w[0].start()
+    for owner in g[1].arrivals():
+        project(owner, 1)
+    publish(1)
+    w[0].forward()
     r2 = resid[...] * resid[...]
     sqown[...] = lax.dot_general(
         jnp.ones((8, cols), F32), r2, (((1,), (1,)), ((), ())),
@@ -367,43 +399,65 @@
         c = rcopy(sqown, squares.at[k], ssend.at[k], srecv.at[k], tp=lax.rem(tp + k, n_tp))
         c.start()
         sent.append(c)
-    w.start()
-    g.drain()
+    w[1].start()
+
+    slot = lax.broadcasted_iota(jnp.int32, (cap, rows), 0).astype(F32)
+
+    def chosen(p):
+        return jnp.where(pos[pl.ds(p, 1), :] == slot, 1.0, 0.0)
+
+    def far_copy(p, sign):
+        return rcopy(
+            outgoing.at[p], rows_in.at[p, :, mine], dsend.at[p], drecv.at[p], sp=order.at(p, sign)
+        )
+
+    def near_copy(p, sign):
+        return rcopy(
+            outwide.at[p - n_far], rows_in.at[p], dsend.at[p], drecv.at[p], sp=order.at(p, sign)
+        )
+
+    def reply(p):
+        return rcopy(answer.at[p], returned.at[p], rsend.at[p], rrecv.at[p], sp=order.at(p, -1))
+
+    def scale_copy(p, sign):
+        return rcopy(smsg.at[p], sgot.at[p], lsend.at[p], lrecv.at[p], sp=order.at(p, sign))
+
+    def dispatch(p):
+        outgoing[p] = jnp.dot(
+            chosen(p).astype(BF16), whole[:, mine], preferred_element_type=F32
+        ).astype(BF16)
+        far_copy(p, 1).start()
+
+    dispatch(0)
     total = sqown[...]
     for k, c in enumerate(sent):
         c.wait()
         total = total + squares[k + 1]
     srow[...] = lax.rsqrt(total / (n_tp * cols) + NORM_EPS)
+
+    def scales(p):
+        return lax.dot_general(
+            srow[...], chosen(p), (((1,), (1,)), ((), ())),
+            precision=EXACT, preferred_element_type=F32,
+        )
+
+    @pl.loop(0, n_sp - 1)
+    def _(p):
+        smsg[p] = scales(p)
+        scale_copy(p, 1).start()
+
+    sgot[n_sp - 1] = scales(n_sp - 1)
+
+    @pl.loop(1, n_far)
+    def _(p):
+        dispatch(p)
+
     scol[...] = lax.dot_general(
         srow[...], jnp.full((8, 128), 0.125, F32), (((0,), (0,)), ((), ())),
         precision=EXACT, preferred_element_type=F32,
     )
-    normed[...] = (resid[...] * scol[:, 0:1] * gain[...]).astype(BF16)
-
-    slot = lax.broadcasted_iota(jnp.int32, (cap, rows), 0).astype(F32)
-
-    def chosen(p):
-        return jnp.where(pos[pl.ds(p, 1), :] == slot, 1.0, 0.0)
-
-    def far_copy(p, sign):
-        return rcopy(
-            outgoing.at[p], rows_in.at[p, :, mine], dsend.at[p], drecv.at[p], sp=order.at(p, sign)
-        )
-
-    def near_copy(p, sign):
-        return rcopy(
-            outwide.at[p - n_far], rows_in.at[p], dsend.at[p], drecv.at[p], sp=order.at(p, sign)
-        )
-
-    def reply(p):
-        return rcopy(answer.at[p], returned.at[p], rsend.at[p], rrecv.at[p], sp=order.at(p, -1))
-
-    @pl.loop(0, n_far)
-    def _(p):
-        outgoing[p] = jnp.dot(
-            chosen(p).astype(BF16), normed[...], preferred_element_type=F32
-        ).astype(BF16)
-        far_copy(p, 1).start()
+    for i in range(2):
+        g[i].drain()
 
     def rows_gather(p):
         def place(owner, part):
@@ -418,21 +472,20 @@
         far_copy(p, -1).wait_recv()
         rows_gather(p).start()
 
-    lead = 2
-    w.forward()
-    for p in range(lead):
-        begin_rows(p)
-    for owner in w.arrivals():
-        pass
+    w[1].forward()
+    begin_rows(0)
+    for i in range(2):
+        for owner in w[i].arrivals():
+            pass
 
     def wide_pick(p):
-        hit = chosen(p)
-        scale = jnp.sum(hit * srow[0:1, :], axis=1, keepdims=True)
-        picked = jnp.dot(hit.astype(BF16), whole[...], preferred_element_type=F32)
-        return (picked * scale).astype(BF16)
-
-    @pl.loop(n_far, n_sp - 1)
-    def _(p):
+        return jnp.dot(
+            chosen(p).astype(BF16), whole[...], preferred_element_type=F32
+        ).astype(BF16)
+
+    @pl.loop(0, direct - 1)
+    def _(i):
+        p = n_sp - 2 - i
         outwide[p - n_far] = wide_pick(p)
         near_copy(p, 1).start()
 
@@ -452,18 +505,8 @@
         def give_part(p):
             return rcopy(psend.at[p], precv.at[p], psem.at[p], prem.at[p], tp=sq.reduce)
 
-        sref = shid.at[:, here]
-        sgive = rcopy(sref, sref, csend.at[0], crecv.at[0], tp=sq.gather)
-        sref = shid.at[:, pl.ds(pl.multiple_of((1 - sq.place) * ff, 128), ff)]
-        stake = rcopy(sref, sref, csend.at[0], crecv.at[0], tp=sq.gather)
-        sgivep = rcopy(spsend, sprecv, qsend.at[0], qrecv.at[0], tp=sq.reduce)
     else:
         here = band(tp)
-
-        def shared_place(owner, part):
-            return shid.at[:, band(owner)]
-
-        shared = Gather(n_tp, shared_place, csend, crecv)
 
         def hidden_gather(p):
             def place(owner, part):
@@ -471,6 +514,12 @@
 
             return Gather(n_tp, place, bsend, brecv, base=p * count)
 
+    def shared_place(owner, part):
+        if part is None:
+            return shid.at[:, band(owner)]
+        return shid.at[:, pl.ds(pl.multiple_of(owner * ff + part * (ff // 2), 128), ff // 2)]
+
+    shared = Gather(n_tp, shared_place, csend, crecv)
     loads[1].wait()
     loads[2].wait()
 
@@ -481,13 +530,11 @@
         s = scol[at, 0:1]
         g = jnp.dot(x, sg[...], preferred_element_type=F32) * s
         u = jnp.dot(x, su[...], preferred_element_type=F32) * s
-        shid[at, here] = (jax.nn.silu(g) * u).astype(BF16)
-
-    if two:
-        sgive.start()
-    else:
-        shared.start()
-    w.drain()
+        shid[at, band(tp)] = (jax.nn.silu(g) * u).astype(BF16)
+
+    shared.start()
+    for i in range(2):
+        w[i].drain()
     for c in loads[3:]:
         c.wait()
     for c in swaps:
@@ -519,74 +566,54 @@
             hit = jnp.where(where == lane, 1.0, 0.0).astype(BF16)
             resid[at, :] += weight * jnp.dot(hit, returned[p], preferred_element_type=F32)
 
+    def turn(s):
+        return jnp.where(s == 0, n_sp - 2, jnp.where(s == n_sp - 1, n_sp - 1, s - 1))
+
     back = 4
 
     @pl.loop(0, n_sp + 3)
     def _(s):
-        @pl.when(s + lead < n_far)
-        def _():
-            begin_rows(s + lead)
+        @pl.when(s < n_sp)
+        def _():
+            p = turn(s)
+
+            @pl.when(p < n_far)
+            def _():
+                for _ in rows_gather(p).arrivals():
+                    pass
+
+            @pl.when((p >= n_far) & (p < n_sp - 1))
+            def _():
+                near_copy(p, -1).wait_recv()
+
+            @pl.when(p < n_sp - 1)
+            def _():
+                scale_copy(p, -1).wait_recv()
+
+            scale = lax.dot_general(
+                sgot[p], jnp.full((8, 128), 0.125, F32), (((0,), (0,)), ((), ())),
+                precision=EXACT, preferred_element_type=F32,
+            )[:, 0:1]
+            x = rows_in[p]
+            g = jnp.dot(x, eg[...], preferred_element_type=F32) * scale
+            u = jnp.dot(x, eu[...], preferred_element_type=F32) * scale
+            hidden[p, :, here] = (jax.nn.silu(g) * u).astype(BF16)
+            if two:
+                give_hidden(p).start()
+            else:
+                hidden_gather(p).start()
+
+        @pl.when(s < n_far)
+        def _():
+            rows_gather(s).forward()
 
         @pl.when(s == 0)
         def _():
-            rows_gather(0).forward()
-
-        @pl.when(s + 1 < n_far)
-        def _():
-            rows_gather(s + 1).forward()
-
-        @pl.when(s < n_sp)
-        def _():
-            @pl.when(s < n_far)
-            def _():
-                for _ in rows_gather(s).arrivals():
-                    pass
-
-            @pl.when((s >= n_far) & (s < n_sp - 1))
-            def _():
-                near_copy(s, -1).wait_recv()
-
-            x = rows_in[s]
-            g = jnp.dot(x, eg[...], preferred_element_type=F32)
-            u = jnp.dot(x, eu[...], preferred_element_type=F32)
-            hidden[s, :, here] = (jax.nn.silu(g) * u).astype(BF16)
-            if two:
-                give_hidden(s).start()
-            else:
-                hidden_gather(s).start()
-
-        if two:
-            @pl.when(s == 1)
-            def _():
-                stake.wait_recv()
-
-                @pl.loop(0, rows // 128)
-                def _(r):
-                    at = pl.ds(pl.multiple_of(r * 128, 128), 128)
-                    h = shid[at, :]
-                    resid[at, :] += jnp.dot(h, sd[0], preferred_element_type=F32)
-                    spsend[at, :] = jnp.dot(h, sd[1], preferred_element_type=F32).astype(BF16)
-
-                sgivep.start()
-
-            @pl.when(s == 3)
-            def _():
-                sgivep.wait_recv()
-                resid[...] += sprecv[...].astype(F32)
-        else:
-            @pl.when(s == 1)
-            def _():
-                for _ in shared.arrivals():
-                    pass
-
-                @pl.loop(0, rows // 128)
-                def _(r):
-                    at = pl.ds(pl.multiple_of(r * 128, 128), 128)
-                    resid[at, :] += jnp.dot(shid[at, :], sd[...], preferred_element_type=F32)
+            shared.forward()
 
         @pl.when((s >= 1) & (s < n_sp + 1))
         def _():
-            p = s - 1
+            p = turn(s - 1)
             if two:
                 take_hidden(p).wait_recv()
                 h = hidden[p]
@@ -603,25 +630,35 @@
         if two:
             @pl.when((s >= 2) & (s < n_sp + 2))
             def _():
-                p = s - 2
+                p = turn(s - 2)
                 give_part(p).wait_recv()
                 answer_with(p, (own[p] + precv[p].astype(F32)).astype(BF16))
 
+        @pl.when(s + 1 < n_far)
+        def _():
+            begin_rows(s + 1)
+
+        @pl.when(s == 3)
+        def _():
+            for _ in shared.arrivals():
+                pass
+
+            @pl.loop(0, rows // 128)
+            def _(r):
+                at = pl.ds(pl.multiple_of(r * 128, 128), 128)
+                resid[at, :] += jnp.dot(shid[at, :], sd[...], preferred_element_type=F32)
+
         @pl.when(s >= back)
         def _():
-            combine(s - back)
+            combine(turn(s - back))
 
     @pl.loop(n_sp + 3 - back, n_sp)
-    def _(p):
-        combine(p)
+    def _(s):
+        combine(turn(s))
 
     out[...] = resid[...].astype(BF16)
 
-    if two:
-        sgive.wait_send()
-        sgivep.wait_send()
-    else:
-        shared.drain()
+    shared.drain()
 
     @pl.loop(0, n_sp)
     def _(p):
@@ -643,6 +680,7 @@
         @pl.when(p < n_sp - 1)
         def _():
             reply(p).wait_send()
+            scale_copy(p, 1).wait_send()
 
 
 def shards(
@@ -680,9 +718,6 @@
     n_far = n_sp - direct
     two = n_tp == 4
     ex = decay_extra.reshape(2, rows, 2 * heads)
-    c = np.arange(chan)
-    which = (c % hw >= wide) * heads + c // hw
-    spread = jnp.asarray((which[None, :] == np.arange(2 * heads)[:, None]).astype(np.float32))
     vm = pl.BlockSpec(memory_space=pltpu.VMEM)
     hbm = pl.BlockSpec(memory_space=pl.ANY)
     sem = pltpu.SemaphoreType.DMA
@@ -690,40 +725,43 @@
     down = (2, 2 * ff, cols) if two else (n_tp * ff, cols)
     hid = 2 * ff if two else n_tp * ff
     V = pltpu.VMEM
-    pairs = [(4,), (2,), (n_sp,), (count,), (n_tp,), (count,), (n_sp,), (n_sp * count,)]
-    pairs += [(n_sp,) if two else (n_sp * count,), (n_sp,), (n_sp,), (1,) if two else (count,), (1,)]
+    pairs = [(2,), (2,), (n_sp,), (2 * count,), (n_tp,), (2 * count,), (n_sp,), (n_sp * count,)]
+    pairs += [(n_sp,) if two else (n_sp * count,), (n_sp,), (n_sp,), (count,), (n_sp,)]
+    ins = (
+        rec_input, gate_input, conv_weight, decay_wide, decay_narrow, input_wide, input_narrow,
+        decay_base, ex, tokens, norm_gain.reshape(1, cols), routes.T, route_weight.T,
+    )
     return pl.pallas_call(
         functools.partial(layer_kernel, n_sp, n_tp, cap, direct),
         name="layer",
         out_shape=jax.ShapeDtypeStruct((rows, cols), BF16),
-        in_specs=[vm] * 14 + [hbm] * 7,
+        in_specs=[hbm] * (len(ins) + 7),
         out_specs=vm,
-        scratch_shapes=[
+        scratch_shapes=[V(a.shape, a.dtype) for a in ins] + [
             V((n_tp, chan, cols), BF16), V(shared_gate.shape, BF16), V(shared_up.shape, BF16),
-            V(expert_gate.shape[1:], BF16), V(expert_up.shape[1:], BF16), V(down, BF16), V(down, BF16),
+            V(expert_gate.shape[1:], BF16), V(expert_up.shape[1:], BF16), V(down, BF16),
+            V((n_tp * ff, cols), BF16),
             V((rows, rows), BF16), V((rows, rows), BF16), V((4, groups, gw, gw), BF16),
-            V((2, rows, 2 * heads), F32),
+            V((2, rows, 6 * heads), BF16),
             V((2, 16, chan), BF16), V((rows, chan), BF16), V((rows, chan), BF16),
             V((2, rows, chan), F32), V((2, rows, chan), F32),
-            V((8, chan), F32), V((n_sp, 8, chan), F32), V((rows, chan), BF16),
+            V((2, 2, chan), F32), V((n_sp, 2, chan), F32), V((rows, chan), BF16),
             V((n_tp, rows, chan), BF16), V((n_tp, 8, rows), F32), V((8, rows), F32),
-            V((rows, cols), F32), V((rows, n_tp * cols), BF16), V((rows, cols), BF16),
-            V((8, rows), F32), V((rows, 128), F32),
+            V((rows, cols), F32), V((rows, n_tp * cols), BF16),
+            V((8, rows), F32), V((rows, 128), F32), V((n_sp, 8, cap), F32), V((n_sp, 8, cap), F32),
             V((n_sp, rows), F32), V((n_sp, rows), F32), V((rows, n_sp), F32), V((rows, n_sp), F32),
             V((n_far, cap, cols), BF16), V((direct - 1, cap, n_tp * cols), BF16),
             V((n_sp, cap, n_tp * cols), BF16), V((n_sp, cap, hid), BF16),
             V((n_sp, cap, cols), F32), V((n_sp, cap, cols), BF16), V((n_sp, cap, cols), BF16),
             V((n_sp, cap, cols), BF16), V((n_sp, cap, cols), BF16),
-            V((rows, hid), BF16), V((rows, cols), BF16), V((rows, cols), BF16),
-            sem((9,)),
+            V((rows, n_tp * ff), BF16),
+            sem((len(ins),)), sem((8,)),
         ] + [sem(s) for s in pairs for _ in range(2)],
         compiler_params=pltpu.CompilerParams(
             collective_id=0, has_side_effects=True, vmem_limit_bytes=60 * 1024 * 1024
         ),
     )(
-        rec_input, gate_input, conv_weight, decay_wide, decay_narrow, input_wide, input_narrow,
-        decay_base, ex, spread, tokens, norm_gain.reshape(1, cols), routes.T, route_weight.T,
-        out_weight.reshape(n_tp, chan, cols), shared_gate, shared_up, expert_gate[0], expert_up[0],
+        *ins, out_weight.reshape(n_tp, chan, cols), shared_gate, shared_up, expert_gate[0], expert_up[0],
         expert_down[0], shared_down,
     )
 

time: 150 us -> 138 us (0.920)
  Pallas kernels: 146 us -> 134 us
    pallas_call x1, Pallas kernels: 146 us -> 134 us  [shards(): pl.pallas_call(functools.partial(layer_kernel, n_sp, n_tp, cap, direct),...]
where the time goes in v2:
time: 138 us; the launch traced here: 137 us
  Pallas kernels  134 us (97%)
  local copies, waits for them, and re-layouts  3.44 us (2%)
    pallas_call x1, Pallas kernels, shards(): pl.pallas_call(functools.partial(layer_kernel, n_sp, n_tp, cap, direct),...  134 us

profile of v2, /device:TPU:0, one launch (start us, length us, event | category | flops | bytes accessed | tf_op | source)
XLA Modules:
  0.0 137.4 jit_solution(15355669477145849112)
XLA Ops:
  0.0 0.8 copy.22
  0.8 0.9 copy.23.h_extra
  1.7 133.9 %layer.1 = bf16[384,512]{1,0:T(8,128)(2,1)} custom-call(bf16[384,768]{1,0:T(8,128)(2,1)} %h_rec.1, bf16[384,768]{1,0:T(8,128)(2,1)} %h_gate.1, bf16[4,768]{1,0:T(4,128)(2,1)} %h_convw.1, bf16[2,4,128,128]{3,2,1,0:T(8,128)(2,1)} %h_dw.1, bf16[2,4,64,64]{3,2,1,0:T(8,128)(2,1)} %h_dn.1, bf16[2,4,128,128]{3,2,1,0:T(8,128)(2,1)} %h_iw.1, ...), custom_call_target="tpu_custom_call" | custom-call | tf_op jit(solution)/shard_map/layer/pallas_call | solution.py:734
  135.6 1.8 %copy.25 = bf16[384,512]{1,0:T(8,128)(2,1)} copy(bf16[384,512]{1,0:T(8,128)(2,1)} %layer.1) | data formatting | bytes 786432

commit v3 on v2

--- a/solution.py
+++ b/solution.py
@@ -228,26 +228,33 @@
     for d in range(2):
         left, terms = extra[d], []
         for _ in range(3):
-            terms.append(left.astype(BF16))
-            left = left - terms[-1].astype(F32)
-        exs[d] = jnp.dot(
-            permt[...], jnp.concatenate(terms, axis=1), preferred_element_type=F32
+            terms.append(left.astype(BF16).astype(F32))
+            left = left - terms[-1]
+        exs[d] = lax.dot_general(
+            permt[...], jnp.concatenate(terms, axis=0).astype(BF16), (((1,), (1,)), ((), ())),
+            preferred_element_type=F32,
         ).astype(BF16)
     gperm[...] = jnp.dot(permt[...], gate[...], preferred_element_type=F32).astype(BF16)
 
+    taps = convw[...].astype(F32)
+
+    def convolve(padded, n):
+        conv = padded[0:n] * taps[0:1, :]
+        for j in range(1, CONV):
+            conv = conv + padded[j : j + n] * taps[j : j + 1, :]
+        return conv.astype(BF16)
+
+    x = rec[...].astype(F32)
+    gap = jnp.zeros((2, chan), F32)
+    mixedp[...] = convolve(jnp.concatenate([gap, x, gap[0:1]], axis=0), rows)
     low.wait()
     high.wait()
-    x = rec[...].astype(F32)
-    taps = convw[...].astype(F32)
     lo = jnp.where(sp > 0, halo[0].astype(F32), 0.0)
     hi = jnp.where(sp < n_sp - 1, halo[1].astype(F32), 0.0)
-    padded = jnp.concatenate([lo[14:16], x, hi[0:1]], axis=0)
-    conv = padded[0:rows] * taps[0:1, :]
-    for j in range(1, CONV):
-        conv = conv + padded[j : j + rows] * taps[j : j + 1, :]
-    cperm[...] = jnp.dot(
-        permt[...], conv.astype(BF16), preferred_element_type=F32
-    ).astype(BF16)
+    first, last = rec[0:32, :].astype(F32), rec[rows - 32 : rows, :].astype(F32)
+    mixedp[0:16, :] = convolve(jnp.concatenate([lo[14:16], first[0:17]], axis=0), 16)
+    mixedp[rows - 16 : rows, :] = convolve(jnp.concatenate([last[14:32], hi[0:1]], axis=0), 16)
+    cperm[...] = jnp.dot(permt[...], mixedp[...], preferred_element_type=F32).astype(BF16)
 
     hw = wide + narrow
     ch = lax.broadcasted_iota(jnp.int32, (6 * heads, chan), 1)
@@ -325,6 +332,12 @@
     post[...] = jnp.transpose(pos[...])
     wtt[...] = jnp.transpose(wts[...])
 
+    @pl.loop(0, rows // 16)
+    def _(r):
+        at = pl.ds(pl.multiple_of(r * 16, 16), 16)
+        bv[0, at, :] = bv[0, at, :] + bv[1, at, :]
+        bv[1, at, :] = jax.nn.gelu(gperm[at, :].astype(F32))
+
     for c in sent:
         c.wait()
     carries = []
@@ -343,9 +356,8 @@
     @pl.loop(0, rows // 16)
     def _(r):
         at = pl.ds(pl.multiple_of(r * 16, 16), 16)
-        total = bv[0, at, :] + av[0, at, :] * carries[0]
-        total = total + (bv[1, at, :] + av[1, at, :] * carries[1])
-        mixedp[at, :] = (total * jax.nn.gelu(gperm[at, :].astype(F32))).astype(BF16)
+        total = bv[0, at, :] + av[0, at, :] * carries[0] + av[1, at, :] * carries[1]
+        mixedp[at, :] = (total * bv[1, at, :]).astype(BF16)
 
     mixed[tp] = jnp.dot(perm[...], mixedp[...], preferred_element_type=F32).astype(BF16)
 
@@ -433,29 +445,39 @@
     for k, c in enumerate(sent):
         c.wait()
         total = total + squares[k + 1]
-    srow[...] = lax.rsqrt(total / (n_tp * cols) + NORM_EPS)
+    w[1].forward()
+    left = lax.rsqrt(total / (n_tp * cols) + NORM_EPS)
+    line = lax.broadcasted_iota(jnp.int32, left.shape, 0)
+    terms = jnp.zeros_like(left)
+    for i in range(3):
+        term = left.astype(BF16).astype(F32)
+        terms = jnp.where(line == i, term, terms)
+        left = left - term
+    srow[...] = jnp.concatenate([terms, jnp.zeros_like(terms)], axis=0).astype(BF16)
 
     def scales(p):
         return lax.dot_general(
-            srow[...], chosen(p), (((1,), (1,)), ((), ())),
-            precision=EXACT, preferred_element_type=F32,
+            srow[...], chosen(p).astype(BF16), (((1,), (1,)), ((), ())),
+            preferred_element_type=F32,
+        ).astype(BF16)
+
+    def column(terms):
+        return lax.dot_general(
+            terms, jnp.ones((16, 128), BF16), (((0,), (0,)), ((), ())), preferred_element_type=F32
         )
 
-    @pl.loop(0, n_sp - 1)
-    def _(p):
+    def tell(p):
         smsg[p] = scales(p)
         scale_copy(p, 1).start()
 
-    sgot[n_sp - 1] = scales(n_sp - 1)
+    tell(0)
 
     @pl.loop(1, n_far)
     def _(p):
+        tell(p)
         dispatch(p)
 
-    scol[...] = lax.dot_general(
-        srow[...], jnp.full((8, 128), 0.125, F32), (((0,), (0,)), ((), ())),
-        precision=EXACT, preferred_element_type=F32,
-    )
+    scol[...] = column(srow[...])
     for i in range(2):
         g[i].drain()
 
@@ -472,71 +494,78 @@
         far_copy(p, -1).wait_recv()
         rows_gather(p).start()
 
-    w[1].forward()
-    begin_rows(0)
-    for i in range(2):
-        for owner in w[i].arrivals():
-            pass
-
-    def wide_pick(p):
-        return jnp.dot(
-            chosen(p).astype(BF16), whole[...], preferred_element_type=F32
-        ).astype(BF16)
-
-    @pl.loop(0, direct - 1)
-    def _(i):
-        p = n_sp - 2 - i
-        outwide[p - n_far] = wide_pick(p)
-        near_copy(p, 1).start()
-
-    rows_in[n_sp - 1] = wide_pick(n_sp - 1)
-
-    if two:
-        here = pl.ds(pl.multiple_of(sq.place * ff, 128), ff)
-
-        def give_hidden(p):
-            ref = hidden.at[p, :, here]
-            return rcopy(ref, ref, bsend.at[p], brecv.at[p], tp=sq.gather)
-
-        def take_hidden(p):
-            ref = hidden.at[p, :, pl.ds(pl.multiple_of((1 - sq.place) * ff, 128), ff)]
-            return rcopy(ref, ref, bsend.at[p], brecv.at[p], tp=sq.gather)
-
-        def give_part(p):
-            return rcopy(psend.at[p], precv.at[p], psem.at[p], prem.at[p], tp=sq.reduce)
-
-    else:
-        here = band(tp)
-
-        def hidden_gather(p):
-            def place(owner, part):
-                return hidden.at[p, :, band(owner)]
-
-            return Gather(n_tp, place, bsend, brecv, base=p * count)
-
-    def shared_place(owner, part):
-        if part is None:
-            return shid.at[:, band(owner)]
-        return shid.at[:, pl.ds(pl.multiple_of(owner * ff + part * (ff // 2), 128), ff // 2)]
-
-    shared = Gather(n_tp, shared_place, csend, crecv)
-    loads[1].wait()
-    loads[2].wait()
-
-    @pl.loop(0, rows // 128)
-    def _(r):
-        at = pl.ds(pl.multiple_of(r * 128, 128), 128)
+    def shared_slot(i):
+        def place(owner, part):
+            at = pl.ds(i * half, half)
+            if part is None:
+                return shid.at[at, band(owner)]
+            return shid.at[at, pl.ds(pl.multiple_of(owner * ff + part * (ff // 2), 128), ff // 2)]
+
+        return place
+
+    shared = [Gather(n_tp, shared_slot(i), csend, crecv, base=i * count) for i in range(2)]
+
+    def shared_units(i):
+        at = pl.ds(i * half, half)
         x = whole[at, :]
         s = scol[at, 0:1]
         g = jnp.dot(x, sg[...], preferred_element_type=F32) * s
         u = jnp.dot(x, su[...], preferred_element_type=F32) * s
         shid[at, band(tp)] = (jax.nn.silu(g) * u).astype(BF16)
-
-    shared.start()
+        shared[i].start()
+
+    for owner in w[0].arrivals():
+        pass
+    for c in loads[1:]:
+        c.wait()
+    shared_units(0)
+    for owner in w[1].arrivals():
+        pass
+
+    def wide_pick(p):
+        return jnp.dot(
+            chosen(p).astype(BF16), whole[...], preferred_element_type=F32
+        ).astype(BF16)
+
+    def near(p):
+        outwide[p - n_far] = wide_pick(p)
+        tell(p)
+        near_copy(p, 1).start()
+
+    if two:
+        here = pl.ds(pl.multiple_of(sq.place * ff, 128), ff)
+
+        def give_hidden(p):
+            ref = hidden.at[p, :, here]
+            return rcopy(ref, ref, bsend.at[p], brecv.at[p], tp=sq.gather)
+
+        def take_hidden(p):
+            ref = hidden.at[p, :, pl.ds(pl.multiple_of((1 - sq.place) * ff, 128), ff)]
+            return rcopy(ref, ref, bsend.at[p], brecv.at[p], tp=sq.gather)
+
+        def give_part(p):
+            return rcopy(psend.at[p], precv.at[p], psem.at[p], prem.at[p], tp=sq.reduce)
+
+    else:
+        here = band(tp)
+
+        def hidden_gather(p):
+            def place(owner, part):
+                return hidden.at[p, :, band(owner)]
+
+            return Gather(n_tp, place, bsend, brecv, base=p * count)
+
+    near(n_sp - 2)
+    shared_units(1)
+
+    @pl.loop(n_far, n_sp - 2)
+    def _(p):
+        near(p)
+
+    rows_in[n_sp - 1] = wide_pick(n_sp - 1)
+    sgot[n_sp - 1] = scales(n_sp - 1)
     for i in range(2):
         w[i].drain()
-    for c in loads[3:]:
-        c.wait()
     for c in swaps:
         c.wait()
 
@@ -555,21 +584,17 @@
         def _():
             reply(p).wait_recv()
 
-        lane = lax.broadcasted_iota(jnp.int32, (128, cap), 1).astype(F32)
-        which = lax.broadcasted_iota(jnp.int32, (128, n_sp), 1) == p
-
-        @pl.loop(0, rows // 128)
-        def _(r):
-            at = pl.ds(pl.multiple_of(r * 128, 128), 128)
-            where = jnp.sum(jnp.where(which, post[at, :], 0.0), axis=1, keepdims=True)
-            weight = jnp.sum(jnp.where(which, wtt[at, :], 0.0), axis=1, keepdims=True)
-            hit = jnp.where(where == lane, 1.0, 0.0).astype(BF16)
-            resid[at, :] += weight * jnp.dot(hit, returned[p], preferred_element_type=F32)
+        which = lax.broadcasted_iota(jnp.int32, (rows, n_sp), 1) == p
+        where = jnp.sum(jnp.where(which, post[...], 0.0), axis=1, keepdims=True)
+        weight = jnp.sum(jnp.where(which, wtt[...], 0.0), axis=1, keepdims=True)
+        lane = lax.broadcasted_iota(jnp.int32, (rows, cap), 1).astype(F32)
+        hit = jnp.where(where == lane, 1.0, 0.0).astype(BF16)
+        resid[...] += weight * jnp.dot(hit, returned[p], preferred_element_type=F32)
 
     def turn(s):
         return jnp.where(s == 0, n_sp - 2, jnp.where(s == n_sp - 1, n_sp - 1, s - 1))
 
-    back = 4
+    back = 5
 
     @pl.loop(0, n_sp + 3)
     def _(s):
@@ -590,10 +615,7 @@
             def _():
                 scale_copy(p, -1).wait_recv()
 
-            scale = lax.dot_general(
-                sgot[p], jnp.full((8, 128), 0.125, F32), (((0,), (0,)), ((), ())),
-                precision=EXACT, preferred_element_type=F32,
-            )[:, 0:1]
+            scale = column(sgot[p])[:, 0:1]
             x = rows_in[p]
             g = jnp.dot(x, eg[...], preferred_element_type=F32) * scale
             u = jnp.dot(x, eu[...], preferred_element_type=F32) * scale
@@ -603,13 +625,16 @@
             else:
                 hidden_gather(p).start()
 
+        @pl.when(s == 0)
+        def _():
+            shared[0].forward()
+            shared[1].forward()
+            begin_rows(0)
+            begin_rows(1)
+
         @pl.when(s < n_far)
         def _():
             rows_gather(s).forward()
-
-        @pl.when(s == 0)
-        def _():
-            shared.forward()
 
         @pl.when((s >= 1) & (s < n_sp + 1))
         def _():
@@ -627,6 +652,10 @@
                     p, jnp.dot(hidden[p], ed[...], preferred_element_type=F32).astype(BF16)
                 )
 
+        @pl.when((s > 0) & (s + 1 < n_far))
+        def _():
+            begin_rows(s + 1)
+
         if two:
             @pl.when((s >= 2) & (s < n_sp + 2))
             def _():
@@ -634,14 +663,11 @@
                 give_part(p).wait_recv()
                 answer_with(p, (own[p] + precv[p].astype(F32)).astype(BF16))
 
-        @pl.when(s + 1 < n_far)
-        def _():
-            begin_rows(s + 1)
-
         @pl.when(s == 3)
         def _():
-            for _ in shared.arrivals():
-                pass
+            for i in range(2):
+                for _ in shared[i].arrivals():
+                    pass
 
             @pl.loop(0, rows // 128)
             def _(r):
@@ -658,7 +684,8 @@
 
     out[...] = resid[...].astype(BF16)
 
-    shared.drain()
+    for i in range(2):
+        shared[i].drain()
 
     @pl.loop(0, n_sp)
     def _(p):
@@ -717,7 +744,7 @@
     direct = 4
     n_far = n_sp - direct
     two = n_tp == 4
-    ex = decay_extra.reshape(2, rows, 2 * heads)
+    ex = decay_extra.transpose(0, 2, 3, 1).reshape(2, 2 * heads, rows)
     vm = pl.BlockSpec(memory_space=pltpu.VMEM)
     hbm = pl.BlockSpec(memory_space=pl.ANY)
     sem = pltpu.SemaphoreType.DMA
@@ -726,7 +753,7 @@
     hid = 2 * ff if two else n_tp * ff
     V = pltpu.VMEM
     pairs = [(2,), (2,), (n_sp,), (2 * count,), (n_tp,), (2 * count,), (n_sp,), (n_sp * count,)]
-    pairs += [(n_sp,) if two else (n_sp * count,), (n_sp,), (n_sp,), (count,), (n_sp,)]
+    pairs += [(n_sp,) if two else (n_sp * count,), (n_sp,), (n_sp,), (2 * count,), (n_sp,)]
     ins = (
         rec_input, gate_input, conv_weight, decay_wide, decay_narrow, input_wide, input_narrow,
         decay_base, ex, tokens, norm_gain.reshape(1, cols), routes.T, route_weight.T,
@@ -748,7 +775,7 @@
             V((2, 2, chan), F32), V((n_sp, 2, chan), F32), V((rows, chan), BF16),
             V((n_tp, rows, chan), BF16), V((n_tp, 8, rows), F32), V((8, rows), F32),
             V((rows, cols), F32), V((rows, n_tp * cols), BF16),
-            V((8, rows), F32), V((rows, 128), F32), V((n_sp, 8, cap), F32), V((n_sp, 8, cap), F32),
+            V((16, rows), BF16), V((rows, 128), F32), V((n_sp, 16, cap), BF16), V((n_sp, 16, cap), BF16),
             V((n_sp, rows), F32), V((n_sp, rows), F32), V((rows, n_sp), F32), V((rows, n_sp), F32),
             V((n_far, cap, cols), BF16), V((direct - 1, cap, n_tp * cols), BF16),
             V((n_sp, cap, n_tp * cols), BF16), V((n_sp, cap, hid), BF16),

time: 138 us -> 130 us (0.942)
  Pallas kernels: 134 us -> 127 us
    pallas_call x1, Pallas kernels: 134 us -> 127 us  [shards(): pl.pallas_call(functools.partial(layer_kernel, n_sp, n_tp, cap, direct),...]
where the time goes in v3:
time: 130 us
  Pallas kernels  127 us (98%)
  local copies, waits for them, and re-layouts  3.12 us (2%)
    pallas_call x1, Pallas kernels, shards(): pl.pallas_call(functools.partial(layer_kernel, n_sp, n_tp, cap, direct),...  127 us

profile of v3, /device:TPU:0, one launch (start us, length us, event | category | flops | bytes accessed | tf_op | source)
XLA Modules:
  0.0 129.7 jit_solution(4497157560256785163)
XLA Ops:
  0.0 1.4 %reshape.9.h_extra = f32[2,8,384]{2,1,0:T(8,128)} reshape(f32[2,2,4,384]{3,2,1,0:T(4,128)} %bitcast.12) | data formatting | bytes 49152 | tf_op jit(solution)/shard_map/reshape | solution.py:747
  1.4 126.5 %layer.1 = bf16[384,512]{1,0:T(8,128)(2,1)} custom-call(bf16[384,768]{1,0:T(8,128)(2,1)} %h_rec.1, bf16[384,768]{1,0:T(8,128)(2,1)} %h_gate.1, bf16[4,768]{1,0:T(4,128)(2,1)} %h_convw.1, bf16[2,4,128,128]{3,2,1,0:T(8,128)(2,1)} %h_dw.1, bf16[2,4,64,64]{3,2,1,0:T(8,128)(2,1)} %h_dn.1, bf16[2,4,128,128]{3,2,1,0:T(8,128)(2,1)} %h_iw.1, ...), custom_call_target="tpu_custom_call" | custom-call | tf_op jit(solution)/shard_map/layer/pallas_call | solution.py:761
  127.9 1.8 %copy.22 = bf16[384,512]{1,0:T(8,128)(2,1)} copy(bf16[384,512]{1,0:T(8,128)(2,1)} %layer.1) | data formatting | bytes 786432

commit v4 on v3

--- a/solution.py
+++ b/solution.py
@@ -555,15 +555,19 @@
 
             return Gather(n_tp, place, bsend, brecv, base=p * count)
 
-    near(n_sp - 2)
-    shared_units(1)
-
     @pl.loop(n_far, n_sp - 2)
     def _(p):
         near(p)
 
+    shared_units(1)
+    shared[0].forward()
+    near(n_sp - 2)
     rows_in[n_sp - 1] = wide_pick(n_sp - 1)
     sgot[n_sp - 1] = scales(n_sp - 1)
+    shared[1].forward()
+    begin_rows(0)
+    begin_rows(1)
+    rows_gather(0).forward()
     for i in range(2):
         w[i].drain()
     for c in swaps:
@@ -591,16 +595,13 @@
         hit = jnp.where(where == lane, 1.0, 0.0).astype(BF16)
         resid[...] += weight * jnp.dot(hit, returned[p], preferred_element_type=F32)
 
-    def turn(s):
-        return jnp.where(s == 0, n_sp - 2, jnp.where(s == n_sp - 1, n_sp - 1, s - 1))
-
     back = 5
 
     @pl.loop(0, n_sp + 3)
     def _(s):
         @pl.when(s < n_sp)
         def _():
-            p = turn(s)
+            p = s
 
             @pl.when(p < n_far)
             def _():
@@ -625,20 +626,13 @@
             else:
                 hidden_gather(p).start()
 
-        @pl.when(s == 0)
-        def _():
-            shared[0].forward()
-            shared[1].forward()
-            begin_rows(0)
-            begin_rows(1)
-
-        @pl.when(s < n_far)
-        def _():
-            rows_gather(s).forward()
+        @pl.when(s + 1 < n_far)
+        def _():
+            rows_gather(s + 1).forward()
 
         @pl.when((s >= 1) & (s < n_sp + 1))
         def _():
-            p = turn(s - 1)
+            p = s - 1
             if two:
                 take_hidden(p).wait_recv()
                 h = hidden[p]
@@ -652,18 +646,18 @@
                     p, jnp.dot(hidden[p], ed[...], preferred_element_type=F32).astype(BF16)
                 )
 
-        @pl.when((s > 0) & (s + 1 < n_far))
-        def _():
-            begin_rows(s + 1)
+        @pl.when(s + 2 < n_far)
+        def _():
+            begin_rows(s + 2)
 
         if two:
             @pl.when((s >= 2) & (s < n_sp + 2))
             def _():
-                p = turn(s - 2)
+                p = s - 2
                 give_part(p).wait_recv()
                 answer_with(p, (own[p] + precv[p].astype(F32)).astype(BF16))
 
-        @pl.when(s == 3)
+        @pl.when(s == 2)
         def _():
             for i in range(2):
                 for _ in shared[i].arrivals():
@@ -676,13 +670,7 @@
 
         @pl.when(s >= back)
         def _():
-            combine(turn(s - back))
-
-    @pl.loop(n_sp + 3 - back, n_sp)
-    def _(s):
-        combine(turn(s))
-
-    out[...] = resid[...].astype(BF16)
+            combine(s - back)
 
     for i in range(2):
         shared[i].drain()
@@ -708,6 +696,12 @@
         def _():
             reply(p).wait_send()
             scale_copy(p, 1).wait_send()
+
+    @pl.loop(n_sp + 3 - back, n_sp)
+    def _(s):
+        combine(s)
+
+    out[...] = resid[...].astype(BF16)
 
 
 def shards(

time: 130 us -> 126 us (0.969)
  Pallas kernels: 127 us -> 123 us
    pallas_call x1, Pallas kernels: 127 us -> 123 us  [shards(): pl.pallas_call(functools.partial(layer_kernel, n_sp, n_tp, cap, direct),...]
where the time goes in v4:
time: 126 us
  Pallas kernels  123 us (98%)
  local copies, waits for them, and re-layouts  3.12 us (2%)
    pallas_call x1, Pallas kernels, shards(): pl.pallas_call(functools.partial(layer_kernel, n_sp, n_tp, cap, direct),...  123 us

profile of v4, /device:TPU:0, one launch (start us, length us, event | category | flops | bytes accessed | tf_op | source)
XLA Modules:
  0.0 125.9 jit_solution(773168124512911623)
XLA Ops:
  0.0 1.4 %reshape.9.h_extra = f32[2,8,384]{2,1,0:T(8,128)} reshape(f32[2,2,4,384]{3,2,1,0:T(4,128)} %bitcast.12) | data formatting | bytes 49152 | tf_op jit(solution)/shard_map/reshape | solution.py:741
  1.4 122.8 %layer.1 = bf16[384,512]{1,0:T(8,128)(2,1)} custom-call(bf16[384,768]{1,0:T(8,128)(2,1)} %h_rec.1, bf16[384,768]{1,0:T(8,128)(2,1)} %h_gate.1, bf16[4,768]{1,0:T(4,128)(2,1)} %h_convw.1, bf16[2,4,128,128]{3,2,1,0:T(8,128)(2,1)} %h_dw.1, bf16[2,4,64,64]{3,2,1,0:T(8,128)(2,1)} %h_dn.1, bf16[2,4,128,128]{3,2,1,0:T(8,128)(2,1)} %h_iw.1, ...), custom_call_target="tpu_custom_call" | custom-call | tf_op jit(solution)/shard_map/layer/pallas_call | solution.py:755
  124.1 1.8 %copy.22 = bf16[384,512]{1,0:T(8,128)(2,1)} copy(bf16[384,512]{1,0:T(8,128)(2,1)} %layer.1) | data formatting | bytes 786432

commit v5 on v4

--- a/solution.py
+++ b/solution.py
@@ -226,7 +226,7 @@
                 wblk[2 * d + k, h // per, a:b, a:b] = w[d, h]
                 wblk[2 * d + k, h // per, b : b + narrow, b : b + narrow] = n[d, h]
     for d in range(2):
-        left, terms = extra[d], []
+        left, terms = jnp.concatenate([extra[d, 0], extra[d, 1]], axis=0), []
         for _ in range(3):
             terms.append(left.astype(BF16).astype(F32))
             left = left - terms[-1]
@@ -261,6 +261,8 @@
     head, within = ch // hw, ch % hw
     term = lax.broadcasted_iota(jnp.int32, (6 * heads, chan), 0) % (2 * heads)
     spread = jnp.where(term == jnp.where(within >= wide, heads, 0) + head, 1.0, 0.0).astype(BF16)
+    cuts = ((0, wide), (wide, gw)) if per == 2 and wide % 128 == 0 else ((0, gw),)
+    pieces = [(g, a, b) for g in range(groups) for a, b in cuts]
     step = rows // 2
 
     @pl.loop(0, rows // step)
@@ -268,11 +270,13 @@
         at = pl.ds(pl.multiple_of(r * step, step), step)
         for d in range(2):
             ex = jnp.dot(exs[d, at, :], spread, preferred_element_type=F32)
-            for g in range(groups):
-                lanes = slice(g * gw, (g + 1) * gw)
+            for g, a, b in pieces:
+                lanes, blk = slice(g * gw + a, g * gw + b), slice(a, b)
                 c = cperm[at, lanes]
-                rate = logistic(jnp.dot(c, wblk[2 * d, g], preferred_element_type=F32))
-                admit = logistic(jnp.dot(c, wblk[2 * d + 1, g], preferred_element_type=F32))
+                rate, admit = (
+                    logistic(jnp.dot(c, wblk[2 * d + k, g, blk, blk], preferred_element_type=F32))
+                    for k in range(2)
+                )
                 ld = jnp.minimum(ex[:, lanes] - rate * (RATE_SCALE * base[d : d + 1, lanes]), 0.0)
                 a = jnp.exp(ld)
                 bv[d, at, lanes] = jnp.sqrt(jnp.tanh(-ld) * (1.0 + a * a)) * admit * c.astype(F32)
@@ -359,8 +363,6 @@
         total = bv[0, at, :] + av[0, at, :] * carries[0] + av[1, at, :] * carries[1]
         mixedp[at, :] = (total * bv[1, at, :]).astype(BF16)
 
-    mixed[tp] = jnp.dot(perm[...], mixedp[...], preferred_element_type=F32).astype(BF16)
-
     half, quarter = rows // 2, rows // 4
 
     def rows_of(i, part):
@@ -385,7 +387,15 @@
         at = pl.ds(i * half, half)
         whole[at, mine] = (resid[at, :] * gain[...]).astype(BF16)
 
+    def unscramble(i):
+        at = pl.ds(i * half, half)
+        mixed[tp, at, :] = jnp.dot(
+            perm[at, :], mixedp[...], preferred_element_type=F32
+        ).astype(BF16)
+
+    unscramble(0)
     g[0].start()
+    unscramble(1)
     resid[...] = tokens[...].astype(F32)
     loads[0].wait()
     project(tp, 0)
@@ -595,36 +605,38 @@
         hit = jnp.where(where == lane, 1.0, 0.0).astype(BF16)
         resid[...] += weight * jnp.dot(hit, returned[p], preferred_element_type=F32)
 
+    def units(p):
+
+        @pl.when(p < n_far)
+        def _():
+            for _ in rows_gather(p).arrivals():
+                pass
+
+        @pl.when((p >= n_far) & (p < n_sp - 1))
+        def _():
+            near_copy(p, -1).wait_recv()
+
+        @pl.when(p < n_sp - 1)
+        def _():
+            scale_copy(p, -1).wait_recv()
+
+        scale = column(sgot[p])[:, 0:1]
+        x = rows_in[p]
+        g = jnp.dot(x, eg[...], preferred_element_type=F32) * scale
+        u = jnp.dot(x, eu[...], preferred_element_type=F32) * scale
+        hidden[p, :, here] = (jax.nn.silu(g) * u).astype(BF16)
+        if two:
+            give_hidden(p).start()
+        else:
+            hidden_gather(p).start()
+
     back = 5
 
     @pl.loop(0, n_sp + 3)
     def _(s):
-        @pl.when(s < n_sp)
-        def _():
-            p = s
-
-            @pl.when(p < n_far)
-            def _():
-                for _ in rows_gather(p).arrivals():
-                    pass
-
-            @pl.when((p >= n_far) & (p < n_sp - 1))
-            def _():
-                near_copy(p, -1).wait_recv()
-
-            @pl.when(p < n_sp - 1)
-            def _():
-                scale_copy(p, -1).wait_recv()
-
-            scale = column(sgot[p])[:, 0:1]
-            x = rows_in[p]
-            g = jnp.dot(x, eg[...], preferred_element_type=F32) * scale
-            u = jnp.dot(x, eu[...], preferred_element_type=F32) * scale
-            hidden[p, :, here] = (jax.nn.silu(g) * u).astype(BF16)
-            if two:
-                give_hidden(p).start()
-            else:
-                hidden_gather(p).start()
+        @pl.when(s <= n_far)
+        def _():
+            units(s)
 
         @pl.when(s + 1 < n_far)
         def _():
@@ -645,6 +657,10 @@
                 answer_with(
                     p, jnp.dot(hidden[p], ed[...], preferred_element_type=F32).astype(BF16)
                 )
+
+        @pl.when((s >= n_far) & (s + 1 < n_sp))
+        def _():
+            units(s + 1)
 
         @pl.when(s + 2 < n_far)
         def _():
@@ -738,7 +754,7 @@
     direct = 4
     n_far = n_sp - direct
     two = n_tp == 4
-    ex = decay_extra.transpose(0, 2, 3, 1).reshape(2, 2 * heads, rows)
+    ex = decay_extra.transpose(0, 2, 3, 1)
     vm = pl.BlockSpec(memory_space=pltpu.VMEM)
     hbm = pl.BlockSpec(memory_space=pl.ANY)
     sem = pltpu.SemaphoreType.DMA
@@ -746,7 +762,7 @@
     down = (2, 2 * ff, cols) if two else (n_tp * ff, cols)
     hid = 2 * ff if two else n_tp * ff
     V = pltpu.VMEM
-    pairs = [(2,), (2,), (n_sp,), (2 * count,), (n_tp,), (2 * count,), (n_sp,), (n_sp * count,)]
+    pairs = [(2,), (2,), (n_sp,), (2 * count,), (n_tp,), (2 * count,), (n_sp,), (n_far * count,)]
     pairs += [(n_sp,) if two else (n_sp * count,), (n_sp,), (n_sp,), (2 * count,), (n_sp,)]
     ins = (
         rec_input, gate_input, conv_weight, decay_wide, decay_narrow, input_wide, input_narrow,

time: 126 us -> 123 us (0.976)
  Pallas kernels: 123 us -> 121 us
  local copies, waits for them, and re-layouts: 3.12 us -> 1.77 us
    pallas_call x1, Pallas kernels: 123 us -> 121 us  [shards(): pl.pallas_call(functools.partial(layer_kernel, n_sp, n_tp, cap, direct),...]
    reshape x1 -> x0, local copies, waits for them, and re-layouts: 1.36 us -> none  [shards(): ex = decay_extra.transpose(0, 2, 3, 1).reshape(2, 2 * heads, rows)]
where the time goes in v5:
time: 123 us
  Pallas kernels  121 us (98%)
  local copies, waits for them, and re-layouts  1.77 us (1%)
    pallas_call x1, Pallas kernels, shards(): pl.pallas_call(functools.partial(layer_kernel, n_sp, n_tp, cap, direct),...  121 us

profile of v5, /device:TPU:0, one launch (start us, length us, event | category | flops | bytes accessed | tf_op | source)
XLA Modules:
  0.0 122.9 jit_solution(14909100892002169659)
XLA Ops:
  0.0 121.2 %layer.1 = bf16[384,512]{1,0:T(8,128)(2,1)} custom-call(bf16[384,768]{1,0:T(8,128)(2,1)} %h_rec.1, bf16[384,768]{1,0:T(8,128)(2,1)} %h_gate.1, bf16[4,768]{1,0:T(4,128)(2,1)} %h_convw.1, bf16[2,4,128,128]{3,2,1,0:T(8,128)(2,1)} %h_dw.1, bf16[2,4,64,64]{3,2,1,0:T(8,128)(2,1)} %h_dn.1, bf16[2,4,128,128]{3,2,1,0:T(8,128)(2,1)} %h_iw.1, ...), custom_call_target="tpu_custom_call" | custom-call | tf_op jit(solution)/shard_map/layer/pallas_call | solution.py:771
  121.2 1.8 %copy.22 = bf16[384,512]{1,0:T(8,128)(2,1)} copy(bf16[384,512]{1,0:T(8,128)(2,1)} %layer.1) | data formatting | bytes 786432

commit v6 on v5

--- a/solution.py
+++ b/solution.py
@@ -576,8 +576,8 @@
     sgot[n_sp - 1] = scales(n_sp - 1)
     shared[1].forward()
     begin_rows(0)
+    rows_gather(0).forward()
     begin_rows(1)
-    rows_gather(0).forward()
     for i in range(2):
         w[i].drain()
     for c in swaps:

time: 123 us -> 121 us (0.984)
    pallas_call x1, Pallas kernels: 121 us -> 120 us  [shards(): pl.pallas_call(functools.partial(layer_kernel, n_sp, n_tp, cap, direct),...]
where the time goes in v6:
time: 121 us
  Pallas kernels  120 us (99%)
  local copies, waits for them, and re-layouts  1.77 us (1%)
    pallas_call x1, Pallas kernels, shards(): pl.pallas_call(functools.partial(layer_kernel, n_sp, n_tp, cap, direct),...  120 us

profile of v6, /device:TPU:0, one launch (start us, length us, event | category | flops | bytes accessed | tf_op | source)
XLA Modules:
  0.0 121.3 jit_solution(9863121637717518901)
XLA Ops:
  0.0 119.5 %layer.1 = bf16[384,512]{1,0:T(8,128)(2,1)} custom-call(bf16[384,768]{1,0:T(8,128)(2,1)} %h_rec.1, bf16[384,768]{1,0:T(8,128)(2,1)} %h_gate.1, bf16[4,768]{1,0:T(4,128)(2,1)} %h_convw.1, bf16[2,4,128,128]{3,2,1,0:T(8,128)(2,1)} %h_dw.1, bf16[2,4,64,64]{3,2,1,0:T(8,128)(2,1)} %h_dn.1, bf16[2,4,128,128]{3,2,1,0:T(8,128)(2,1)} %h_iw.1, ...), custom_call_target="tpu_custom_call" | custom-call | tf_op jit(solution)/shard_map/layer/pallas_call | solution.py:771
  119.5 1.8 %copy.22 = bf16[384,512]{1,0:T(8,128)(2,1)} copy(bf16[384,512]{1,0:T(8,128)(2,1)} %layer.1) | data formatting | bytes 786432
